TPU v7x, 32 devices: a whole 2x2x4 slice. The times are simulated.
32 devices in a mesh: sp: 8 (over z, y), tp: 4 (over x, core).
Axes of the slice: x: 2, y: 2, z: 4, core: 2. Of those that a mesh axis runs over, the one named last changes fastest.
Arguments:
- queries: bfloat16 [8192, 1024], P('sp', 'tp'), may hold values from -6 to 6
- keys: bfloat16 [8192, 1024], P('sp', 'tp'), may hold values from -6 to 6
- values: bfloat16 [8192, 1024], P('sp', 'tp'), may hold values from -6 to 6
- gates: bfloat16 [8192, 1024], P('sp', 'tp'), may hold values from -6 to 6
- log_decay: float32 [8192, 8], P('sp', 'tp'), may hold values from -1.6 to 0, as said below
- norm_gain: float32 [8, 128], P('tp'), may hold values from 0.1 to 1.9
- out_weight: bfloat16 [1024, 2048], P('tp'), may hold values from -0.1875 to 0.1875
- resid: bfloat16 [8192, 2048], P(('sp', 'tp')), may hold values from -6 to 6
- post_mix_gain: float32 [2048], replicated, may hold values from 0.1 to 1.9
- pre_ffn_gain: float32 [2048], replicated, may hold values from 0.1 to 1.9
- w_gate: bfloat16 [2048, 5632], P('sp', 'tp'), may hold values from -0.125 to 0.125
- w_up: bfloat16 [2048, 5632], P('sp', 'tp'), may hold values from -0.125 to 0.125
- w_down: bfloat16 [5632, 2048], P('tp', 'sp'), may hold values from -0.078125 to 0.078125
- post_ffn_gain: float32 [2048], replicated, may hold values from 0.1 to 1.9
Outputs:
- updated: bfloat16 [8192, 2048], P(('sp', 'tp'))
Inputs may be any that keep to these rules, and one draw needn't show every extreme that they name: `log_decay`: every entry is negative.
All inputs are finite; a program needn't handle non-finite values.
Results may differ from a plain program's by a relative error of at most 0.02.
Values may be sent and summed in bfloat16 or wider, within the bound.
A program may use at most 128 MiB of HBM per device.

v0:
```python
import jax
import jax.numpy as jnp
from jax import lax
from jax.sharding import PartitionSpec as P

BLOCK = 512


EPSILON = 1e-06


def entering(x, axis, join, neutral):
    place = lax.axis_index(axis)
    gathered = jax.tree.map(
        lambda a, kind: lax.all_gather(a.astype(kind), axis), x, (jnp.bfloat16, jnp.bfloat16)
    )
    state = jax.tree.map(lambda a, e: jnp.zeros_like(a) + jnp.asarray(e, a.dtype), x, neutral)

    def one(step, state):
        return join(
            state,
            jax.tree.map(
                lambda a, own: lax.dynamic_index_in_dim(a, step, 0, False).astype(own.dtype),
                gathered,
                x,
            ),
        )

    return lax.fori_loop(0, place, one, state)


def rms_norm(values_in, gain_vec):
    widened = values_in.astype(jnp.float32)
    return (
        widened
        * lax.rsqrt(jnp.mean(widened * widened, axis=-1, keepdims=True) + EPSILON)
        * gain_vec
    )


def block_step(carried, pieces):
    query_blk, key_blk, value_blk, decay_blk = pieces
    length = query_blk.shape[1]
    key_scale = query_blk.shape[2] ** (-0.5)
    cumulative = jnp.cumsum(decay_blk, axis=1)
    log_gap = cumulative[:, :, None] - cumulative[:, None, :]
    causal = lax.broadcasted_iota(jnp.int32, (length, length), 0) >= lax.broadcasted_iota(
        jnp.int32, (length, length), 1
    )
    weight = jnp.where(causal[None], jnp.exp(jnp.minimum(log_gap, 0.0)), 0.0)
    products = jnp.einsum("htd,hsd->hts", query_blk, key_blk, preferred_element_type=jnp.float32)
    scores = (products * key_scale * weight).astype(jnp.bfloat16)
    within = jnp.einsum("hts,hsd->htd", scores, value_blk, preferred_element_type=jnp.float32)
    carried_term = (
        jnp.einsum(
            "htd,hde->hte", query_blk.astype(jnp.float32), carried, precision=lax.Precision.HIGHEST
        )
        * jnp.exp(cumulative)[:, :, None]
    )
    to_end = jnp.exp(cumulative[:, -1:] - cumulative) * key_scale
    scaled_keys = (key_blk.astype(jnp.float32) * to_end[:, :, None]).astype(jnp.bfloat16)
    added = jnp.einsum("hsd,hse->hde", scaled_keys, value_blk, preferred_element_type=jnp.float32)
    carried = jnp.exp(cumulative[:, -1])[:, None, None] * carried + added
    return (carried, within + carried_term)


def to_blocks(matrix, block_len, head_count):
    row_count = matrix.shape[0]
    return matrix.reshape(row_count // block_len, block_len, head_count, -1).transpose(0, 2, 1, 3)


def finish_heads(retention, gates, norm_gain):
    centered = retention - jnp.mean(retention, axis=-1, keepdims=True)
    variance = jnp.mean(centered * centered, axis=-1, keepdims=True)
    normed = centered * lax.rsqrt(variance + EPSILON) * norm_gain[None]
    gate_vals = gates.astype(jnp.float32).reshape(normed.shape)
    return (jax.nn.silu(gate_vals) * normed).reshape(normed.shape[0], -1).astype(jnp.bfloat16)


def combine_states(earlier, later):
    return (earlier[0] * later[0], later[0][:, None, None] * earlier[1] + later[1])


def per_device(
    queries,
    keys,
    values,
    gates,
    log_decay,
    norm_gain,
    out_weight,
    resid,
    post_mix_gain,
    pre_ffn_gain,
    w_gate,
    w_up,
    w_down,
    post_ffn_gain,
):
    row_count = queries.shape[0]
    head_count = log_decay.shape[1]
    head_dim = queries.shape[1] // head_count
    block_count = row_count // BLOCK
    query_blocks = to_blocks(queries, BLOCK, head_count)
    key_blocks = to_blocks(keys, BLOCK, head_count)
    value_blocks = to_blocks(values, BLOCK, head_count)
    decay_blocks = log_decay.reshape(block_count, BLOCK, head_count).transpose(0, 2, 1)
    start_state = jnp.zeros((head_count, head_dim, head_dim), jnp.float32)
    local_state, outputs = lax.scan(
        block_step, start_state, (query_blocks, key_blocks, value_blocks, decay_blocks)
    )
    retention = outputs.transpose(0, 2, 1, 3).reshape(row_count, head_count, head_dim)
    cumulative = jnp.cumsum(log_decay, axis=0)
    local_decay = jnp.exp(cumulative[-1])
    identity = (jnp.ones_like(local_decay), jnp.zeros_like(local_state))
    incoming = entering((local_decay, local_state), "sp", combine_states, identity)
    query_rows = queries.reshape(row_count, head_count, head_dim).astype(jnp.float32)
    retention = (
        retention
        + jnp.einsum("thd,hde->the", query_rows, incoming[1], precision=lax.Precision.HIGHEST)
        * jnp.exp(cumulative)[:, :, None]
    )
    retained = finish_heads(retention, gates, norm_gain)
    quarter = resid.shape[0]
    regrouped = lax.all_to_all(retained, "tp", split_axis=0, concat_axis=1, tiled=True)
    group_rows = out_weight.shape[0]
    empty_mix = jnp.zeros((quarter, out_weight.shape[1]), jnp.float32)
    running = empty_mix
    shard_piece = lax.all_gather(out_weight, "tp", axis=0, tiled=True)
    for offset in range(shard_piece.shape[0] // group_rows):
        columns = lax.dynamic_slice_in_dim(regrouped, offset * group_rows, group_rows, 1)
        part = jnp.dot(
            columns,
            shard_piece[offset * group_rows : (offset + 1) * group_rows],
            preferred_element_type=jnp.float32,
        )
        running = running + part.astype(jnp.bfloat16).astype(jnp.float32)
    mixed = running
    mixed = mixed.astype(jnp.bfloat16)
    middle = (resid.astype(jnp.float32) + rms_norm(mixed, post_mix_gain)).astype(jnp.bfloat16)
    ffn_input = rms_norm(middle, pre_ffn_gain).astype(jnp.bfloat16)
    gathered = lax.all_gather(ffn_input, "tp", axis=0, tiled=True)
    columns = gathered
    gate_act = jnp.dot(
        columns,
        lax.all_gather(w_gate, "sp", axis=0, tiled=True),
        preferred_element_type=jnp.float32,
    )
    up_act = jnp.dot(
        columns, lax.all_gather(w_up, "sp", axis=0, tiled=True), preferred_element_type=jnp.float32
    )
    down_full = lax.all_gather(w_down, "sp", axis=1, tiled=True)
    hidden = (jax.nn.silu(gate_act) * up_act).astype(jnp.bfloat16)
    branch = lax.psum_scatter(
        jnp.dot(hidden, down_full, preferred_element_type=jnp.float32)
        .astype(jnp.bfloat16)
        .astype(jnp.float32)
        .astype(jnp.bfloat16),
        "tp",
        scatter_dimension=0,
        tiled=True,
    )
    return (middle.astype(jnp.float32) + rms_norm(branch, post_ffn_gain)).astype(jnp.bfloat16)


def solution(mesh):
    in_specs = (
        P("sp", "tp"),
        P("sp", "tp"),
        P("sp", "tp"),
        P("sp", "tp"),
        P("sp", "tp"),
        P("tp", None),
        P("tp", None),
        P(("sp", "tp"), None),
        P(),
        P(),
        P("sp", "tp"),
        P("sp", "tp"),
        P("tp", "sp"),
        P(),
    )
    out_specs = P(("sp", "tp"), None)
    return jax.shard_map(
        per_device, mesh=mesh, in_specs=in_specs, out_specs=out_specs, check_vma=False
    )
```

profile of v0, /device:TPU:0, one launch (start us, length us, event | category | flops | bytes accessed | tf_op | source)
XLA Modules:
  0.0 438.4 jit_solution(6785753459974340258)
XLA Ops:
  6.5 0.7 all-gather.8.cloned.1.call-update
  7.3 0.7 all-gather.12.cloned.1.call-update
  8.1 0.7 copy.104
  8.8 0.6 reduce-window.16
  10.0 22.3 %all-gather.1 = bf16[8,1,2]{2,1,0:T(2,128)(2,1)S(1)} all-gather(bf16[1,1,2]{2,1,0:T(2,128)(2,1)S(1)} %bitcast.154), channel_id=1, replica_groups=mesh['sp'=8,'tp'=4] {'sp'}, dimensions={0}, use_global_device_ids=true | all-gather | bytes 36 | tf_op jit(solution)/shard_map/all_gather | solution.py:15
  32.8 9.6 %while.26 = (s32[]{:T(128)}, f32[2,128,128]{2,1,0:T(8,128)S(1)}, f32[2,2,512,128]{3,2,1,0:T(8,128)}, f32[2,2,512]{2,1,0:T(2,128)S(1)}, bf16[2,2,512,128]{3,1,2,0...) while((s32[]{:T(128)}, f32[2,128,128]{2,1,0:T(8,128)S(1)}, ...), condition=%wide.region_3.4_spmd.clone, body=%wide.region_0.3_spmd.clone.sunk | while | flops 507643936 | bytes 5702508 | solution.py:109
  32.8 0.6 reduce-window.26
  34.5 1.0 fusion.75
  35.8 1.2 fusion.76
  37.6 0.6 reduce-window.26
  39.3 1.0 fusion.75
  40.6 1.2 fusion.76
  42.4 1.6 copy.57
  44.1 0.9 reshape.175
  45.2 33.1 %all-gather = bf16[16,128,128]{2,1,0:T(8,128)(2,1)S(1)} all-gather(bf16[2,128,128]{2,1,0:T(8,128)(2,1)S(1)} %convert_element_type.103), channel_id=2, replica_groups=mesh['sp'=8,'tp'=4] {'sp'}, dimensions={0}, use_global_device_ids=true | all-gather | bytes 589824 | tf_op jit(solution)/shard_map/all_gather | solution.py:15
  78.4 0.7 fusion.51
  80.1 11.4 %all_to_all.16 = bf16[4,256,256]{1,2,0:T(8,128)(2,1)S(1)} all-to-all(bf16[4,256,256]{1,2,0:T(8,128)(2,1)S(1)} %copy.62), channel_id=1, replica_groups=mesh['sp'=8,'tp'=4] {'tp'}, dimensions={0} | all-to-all | bytes 1048576 | tf_op jit(solution)/shard_map/all_to_all | solution.py:125
  91.5 1.8 fusion.22
  93.4 1.7 fusion.23
  95.6 0.8 fusion.25
  96.8 0.6 fusion.31
  97.4 1.3 fusion.33
  99.4 0.5 all-gather.16.cloned.1.call-update
  100.1 41.9 %all-gather.12.cloned.1.call-done = bf16[2048,1408]{1,0:T(8,128)(2,1)} async-done(((bf16[256,1408]{1,0:T(8,128)(2,1)}), bf16[2048,1408]{1,0:T(8,128)(2,1)}) %all-gather.12.cloned.1.call-update) | async-done | bytes 5767184 | tf_op jit(solution)/shard_map/all_gather | solution.py:146
  142.0 34.2 %all-gather.10.cloned.1.call-done = bf16[1024,2048]{1,0:T(8,128)(2,1)} async-done(((bf16[256,2048]{1,0:T(8,128)(2,1)}), bf16[1024,2048]{1,0:T(8,128)(2,1)}) %all-gather.10.cloned.1.call-update) | async-done | bytes 4194320 | tf_op jit(solution)/shard_map/all_gather | solution.py:142
  176.3 11.7 %fusion.52 = f32[1024,1408]{1,0:T(8,128)} fusion(bf16[1024,2048]{1,0:T(8,128)(2,1)} %all-gather.10.cloned.1.call-done, bf16[2048,1408]{1,0:T(8,128)(2,1)} %all-gather.12.cloned.1.call-done), kind=kOutput, calls=%fused_computation.97 | convolution fusion | flops 5905580032 | bytes 15728640 | tf_op jit(solution)/shard_map/dot_general | solution.py:144
  188.0 82.7 %all-gather.14.cloned.1.call-done = bf16[2048,1408]{1,0:T(8,128)(2,1)} async-done(((bf16[256,1408]{1,0:T(8,128)(2,1)}), bf16[2048,1408]{1,0:T(8,128)(2,1)}) %all-gather.14.cloned.1.call-update) | async-done | bytes 5767184 | tf_op jit(solution)/shard_map/all_gather | solution.py:150
  270.7 93.2 %all-gather.16.cloned.1.call-done = bf16[1408,2048]{1,0:T(8,128)(2,1)} async-done(((bf16[1408,256]{1,0:T(8,128)(2,1)}), bf16[1408,2048]{1,0:T(8,128)(2,1)}) %all-gather.16.cloned.1.call-update) | async-done | bytes 5767184 | tf_op jit(solution)/shard_map/all_gather | solution.py:152
  363.9 20.5 %convolution_convert_fusion = bf16[1024,2048]{1,0:T(8,128)(2,1)} fusion(bf16[1408,2048]{1,0:T(8,128)(2,1)} %all-gather.16.cloned.1.call-done, f32[1024,1408]{1,0:T(8,128)} %fusion.52, bf16[1024,2048]{1,0:T(8,128)(2,1)} %all-gather.10.cloned.1.call-done, bf16[2048,1408]{1,0:T(8,128)(2,1)} %all-gather.14.cloned.1.call-done), kind=kOutput, calls=%fused_computation.38 | convolution fusion | flops 11821907968 | bytes 25690112 | tf_op jit(solution)/shard_map/dot_general | solution.py:155
  384.5 42.9 %reduce-scatter.2.cloned.1.call-done = bf16[256,2048]{1,0:T(8,128)(2,1)} async-done(((bf16[1024,2048]{1,0:T(8,128)(2,1)}), bf16[256,2048]{1,0:T(8,128)(2,1)}) %reduce-scatter.2.cloned.1.call-update) | async-done | bytes 1048592 | tf_op jit(solution)/shard_map/reduce_scatter | solution.py:154
  427.4 1.5 fusion.29
  428.9 2.6 fusion.34
  (88 shorter events, 7.9 us)
Async XLA Ops:
  6.5 25.8 %copy-start.5 = (bf16[1024,256]{1,0:T(8,128)(2,1)S(1)}, bf16[1024,256]{1,0:T(8,128)(2,1)}, u32[]{:S(2)}) copy-start(bf16[1024,256]{1,0:T(8,128)(2,1)} %param.19) | copy-start | bytes 1572868
  6.5 26.0 %copy-start.6 = (bf16[1024,256]{1,0:T(8,128)(2,1)S(1)}, bf16[1024,256]{1,0:T(8,128)(2,1)}, u32[]{:S(2)}) copy-start(bf16[1024,256]{1,0:T(8,128)(2,1)} %param.20) | copy-start | bytes 1572868
  6.5 26.1 %copy-start.1 = (bf16[1024,256]{1,0:T(8,128)(2,1)S(1)}, bf16[1024,256]{1,0:T(8,128)(2,1)}, u32[]{:S(2)}) copy-start(bf16[1024,256]{1,0:T(8,128)(2,1)} %param.18) | copy-start | bytes 1572868
  6.5 85.0 %all-gather.8.cloned.1.call-start = ((), (), s32[]{:S(2)}) async-start(), calls=%async_computation.2 | async-start | bytes 5242880 | tf_op jit(solution)/shard_map/all_gather | solution.py:129
  7.3 25.5 %copy-start.7 = (f32[1024,2]{0,1:T(2,128)S(1)}, f32[1024,2]{0,1:T(2,128)}, u32[]{:S(2)}) copy-start(f32[1024,2]{0,1:T(2,128)} %param.22) | copy-start | bytes 24580
  7.3 134.8 %all-gather.12.cloned.1.call-start = ((), (), s32[]{:S(2)}) async-start(), calls=%async_computation.4 | async-start | bytes 6488064 | tf_op jit(solution)/shard_map/all_gather | solution.py:146
  8.0 168.3 %all-gather.10.cloned.1.call-start = ((), (), s32[]{:S(2)}) async-start(), calls=%async_computation.3 | async-start | bytes 5242880 | tf_op jit(solution)/shard_map/all_gather | solution.py:142
  42.4 2.6 copy-start.4
  45.0 33.4 %copy-start.2 = (bf16[1024,256]{1,0:T(8,128)(2,1)S(1)}, bf16[1024,256]{1,0:T(8,128)(2,1)}, u32[]{:S(2)}) copy-start(bf16[1024,256]{1,0:T(8,128)(2,1)} %param.18) | copy-start | bytes 1572868
  78.3 0.9 copy-start.11
  91.5 3.5 copy-start
  95.5 1.2 copy-start.3
  95.5 1.2 copy-start.8
  96.4 1.1 copy-start.9
  98.7 171.9 %all-gather.14.cloned.1.call-start = ((), (), s32[]{:S(2)}) async-start(), calls=%async_computation.5 | async-start | bytes 6488064 | tf_op jit(solution)/shard_map/all_gather | solution.py:150
  99.3 264.6 %all-gather.16.cloned.1.call-start = ((), (), s32[]{:S(2)}) async-start(), calls=%async_computation.6 | async-start | bytes 6488064 | tf_op jit(solution)/shard_map/all_gather | solution.py:152
  99.9 327.5 %reduce-scatter.2.cloned.1.call-start = ((), (), s32[]{:S(2)}) async-start(), calls=%async_computation.7 | async-start | bytes 5242880 | tf_op jit(solution)/shard_map/reduce_scatter | solution.py:154
  384.4 44.5 %copy-start.10 = (f32[2048]{0:T(1024)S(1)}, f32[2048]{0:T(1024)}, u32[]{:S(2)}) copy-start(f32[2048]{0:T(1024)} %param.31) | copy-start | bytes 24580
Sparse Core Ops, SparseCore 0:
  8.9 37.1 all-gather.7
  48.3 93.7 all-gather.11
  143.6 32.6 all-gather.9
  178.3 92.3 all-gather.13
  272.6 91.2 all-gather.15
  384.6 42.7 reduce-scatter.1
where the time goes:
time: 439 us; the launch traced here: 438 us
  waiting for transfers between devices  297 us (68%)
  blocking collectives  66.8 us (15%)
  matrix products  43.3 us (10%)
  between operations  13.8 us (3%)
  other arithmetic  9.76 us (2%)
  local copies, waits for them, and re-layouts  6.82 us (2%)
    all_gather x1, waiting for transfers between devices, per_device(): down_full = lax.all_gather(w_down, 'sp', axis=1, tiled=True)  93.2 us
    all_gather x1, waiting for transfers between devices, per_device(): lax.all_gather(w_up, 'sp', axis=0, tiled=True)  82.7 us
    all_gather x2, blocking collectives, entering(): lax.all_gather(a.astype(kind), axis)  55.4 us
    reduce_scatter x1, waiting for transfers between devices, per_device(): lax.psum_scatter(jnp.dot(hidden, down_full, preferred_element_type=jnp.fl...  42.9 us
    all_gather x1, waiting for transfers between devices, per_device(): lax.all_gather(w_gate, 'sp', axis=0, tiled=True)  41.9 us
    all_gather x1, waiting for transfers between devices, per_device(): gathered = lax.all_gather(ffn_input, 'tp', axis=0, tiled=True)  34.2 us
    dot_general x1, matrix products, per_device(): jnp.dot(hidden, down_full, preferred_element_type=jnp.float32)  20.5 us
    dot_general x1, matrix products, per_device(): jnp.dot(columns, lax.all_gather(w_gate, 'sp', axis=0, tiled=True), prefer...  11.7 us
  transfers between devices with their start and end apart: 6, of which 5 were waited for; matrix products, arithmetic and copies ran while one was open for 8% of the time, Pallas kernels for 0%

commit v1 on v0

--- a/solution.py
+++ b/solution.py
@@ -3,30 +3,80 @@
 from jax import lax
 from jax.sharding import PartitionSpec as P
 
+
 BLOCK = 512
 
 
 EPSILON = 1e-06
-
-
-def entering(x, axis, join, neutral):
-    place = lax.axis_index(axis)
-    gathered = jax.tree.map(
-        lambda a, kind: lax.all_gather(a.astype(kind), axis), x, (jnp.bfloat16, jnp.bfloat16)
-    )
-    state = jax.tree.map(lambda a, e: jnp.zeros_like(a) + jnp.asarray(e, a.dtype), x, neutral)
-
-    def one(step, state):
-        return join(
-            state,
-            jax.tree.map(
-                lambda a, own: lax.dynamic_index_in_dim(a, step, 0, False).astype(own.dtype),
-                gathered,
-                x,
-            ),
-        )
-
-    return lax.fori_loop(0, place, one, state)
+LONGEST_RING = 8
+
+
+def entering(decay, state):
+    place = lax.axis_index("sp")
+    head_count, head_dim, _ = state.shape
+    decay_rows = jnp.broadcast_to(decay[:, None, None], (head_count, 16, head_dim))
+    packed = jnp.concatenate([state, decay_rows], axis=1).astype(jnp.bfloat16)
+    gathered = lax.all_gather(packed, "sp")
+
+    def one(step, running):
+        piece = lax.dynamic_index_in_dim(gathered, step, 0, False).astype(jnp.float32)
+        return piece[:, head_dim : head_dim + 1, :] * running + piece[:, :head_dim]
+
+    return lax.fori_loop(0, place, one, jnp.zeros_like(state))
+
+
+def from_earlier(packed, distance):
+    count = lax.axis_size("sp")
+    return lax.ppermute(packed, "sp", [(i, i + distance) for i in range(count - distance)])
+
+
+def entering_by_hops(decay, state):
+    count = lax.axis_size("sp")
+    head_count, head_dim, _ = state.shape
+    decay_rows = jnp.broadcast_to(decay[:, None, None], (head_count, 8, head_dim))
+    packed = jnp.concatenate([state, decay_rows], axis=1)
+    near = from_earlier(packed, 1)
+    far = from_earlier(packed, 2)
+    factor = near[:, head_dim:]
+    pair = jnp.concatenate(
+        [factor[:, :1] * far[:, :head_dim] + near[:, :head_dim], factor * far[:, head_dim:]],
+        axis=1,
+    )
+    total, factor = pair[:, :head_dim], pair[:, head_dim : head_dim + 1]
+    for piece in [from_earlier(pair, distance) for distance in range(2, count, 2)]:
+        total = total + factor * piece[:, :head_dim]
+        factor = factor * piece[:, head_dim : head_dim + 1]
+    return total
+
+
+def ring_order(count):
+    return list(range(0, count, 2)) + list(range(1, count, 2))[::-1]
+
+
+def ring_gather(block, forward_steps, backward_steps):
+    count = lax.axis_size("sp")
+    order = ring_order(count)
+    ahead = [(order[i], order[(i + 1) % count]) for i in range(count)]
+    behind = [(b, a) for a, b in ahead]
+    arrived = [(0, block)]
+    up, down = block, block
+    for step in range(1, max(forward_steps, backward_steps) + 1):
+        if step <= forward_steps:
+            up = lax.ppermute(up, "sp", ahead)
+            arrived.append((-step, up))
+        if step <= backward_steps:
+            down = lax.ppermute(down, "sp", behind)
+            arrived.append((step, down))
+    return arrived
+
+
+def owner_of(offset):
+    count = lax.axis_size("sp")
+    me = lax.axis_index("sp")
+    half = (count + 1) // 2
+    position = jnp.where(me % 2 == 0, me // 2, count - 1 - me // 2)
+    there = (position + offset + count) % count
+    return jnp.where(there < half, 2 * there, 2 * (count - 1 - there) + 1)
 
 
 def rms_norm(values_in, gain_vec):
@@ -77,8 +127,48 @@
     return (jax.nn.silu(gate_vals) * normed).reshape(normed.shape[0], -1).astype(jnp.bfloat16)
 
 
-def combine_states(earlier, later):
-    return (earlier[0] * later[0], later[0][:, None, None] * earlier[1] + later[1])
+def ring_feed_forward(rows, gate_blocks, up_blocks, down_blocks, shape):
+    depth = gate_blocks[0][1].shape[0]
+    width = down_blocks[0][1].shape[1]
+    half = (len(gate_blocks) + 1) // 2
+
+    def project(blocks):
+        total = None
+        for some in (blocks[:half], blocks[half:]):
+            if not some:
+                continue
+            columns = jnp.concatenate(
+                [
+                    lax.dynamic_slice_in_dim(rows, owner_of(offset) * depth, depth, 1)
+                    for offset, _ in some
+                ],
+                axis=1,
+            )
+            weight = jnp.concatenate([block for _, block in some], axis=0)
+            part = jnp.dot(columns, weight, preferred_element_type=jnp.float32)
+            total = part if total is None else total + part
+        return total
+
+    gate_act = project(gate_blocks)
+    up_act = project(up_blocks)
+    hidden = (jax.nn.silu(gate_act) * up_act).astype(jnp.bfloat16)
+    branch = jnp.zeros(shape, jnp.bfloat16)
+    for part_no, some in enumerate((down_blocks[:half], down_blocks[half:])):
+        if not some:
+            continue
+        wide = jnp.concatenate([block for _, block in some], axis=1)
+        part = jnp.dot(hidden, wide, preferred_element_type=jnp.float32).astype(jnp.bfloat16)
+        if part_no == 0:
+            piece = lax.psum_scatter(part, "tp", scatter_dimension=0, tiled=True)
+        else:
+            shares = part.reshape(lax.axis_size("tp"), shape[0], -1)
+            shares = lax.all_to_all(shares, "tp", split_axis=0, concat_axis=0, tiled=True)
+            piece = jnp.sum(shares.astype(jnp.float32), axis=0).astype(jnp.bfloat16)
+        for slot, (offset, _) in enumerate(some):
+            branch = lax.dynamic_update_slice_in_dim(
+                branch, piece[:, slot * width : (slot + 1) * width], owner_of(offset) * width, 1
+            )
+    return branch
 
 
 def per_device(
@@ -97,6 +187,14 @@
     w_down,
     post_ffn_gain,
 ):
+    ring = lax.axis_size("sp")
+    fewer = (ring - 1) // 2
+    more = ring - 1 - fewer
+    short = ring <= LONGEST_RING
+    if short:
+        gate_blocks = ring_gather(w_gate, more, fewer)
+        up_blocks = ring_gather(w_up, fewer, more)
+        down_blocks = ring_gather(w_down, more, fewer)
     row_count = queries.shape[0]
     head_count = log_decay.shape[1]
     head_dim = queries.shape[1] // head_count
@@ -112,12 +210,11 @@
     retention = outputs.transpose(0, 2, 1, 3).reshape(row_count, head_count, head_dim)
     cumulative = jnp.cumsum(log_decay, axis=0)
     local_decay = jnp.exp(cumulative[-1])
-    identity = (jnp.ones_like(local_decay), jnp.zeros_like(local_state))
-    incoming = entering((local_decay, local_state), "sp", combine_states, identity)
+    incoming = (entering_by_hops if short else entering)(local_decay, local_state)
     query_rows = queries.reshape(row_count, head_count, head_dim).astype(jnp.float32)
     retention = (
         retention
-        + jnp.einsum("thd,hde->the", query_rows, incoming[1], precision=lax.Precision.HIGHEST)
+        + jnp.einsum("thd,hde->the", query_rows, incoming, precision=lax.Precision.HIGHEST)
         * jnp.exp(cumulative)[:, :, None]
     )
     retained = finish_heads(retention, gates, norm_gain)
@@ -140,26 +237,25 @@
     middle = (resid.astype(jnp.float32) + rms_norm(mixed, post_mix_gain)).astype(jnp.bfloat16)
     ffn_input = rms_norm(middle, pre_ffn_gain).astype(jnp.bfloat16)
     gathered = lax.all_gather(ffn_input, "tp", axis=0, tiled=True)
-    columns = gathered
-    gate_act = jnp.dot(
-        columns,
-        lax.all_gather(w_gate, "sp", axis=0, tiled=True),
-        preferred_element_type=jnp.float32,
-    )
-    up_act = jnp.dot(
-        columns, lax.all_gather(w_up, "sp", axis=0, tiled=True), preferred_element_type=jnp.float32
-    )
-    down_full = lax.all_gather(w_down, "sp", axis=1, tiled=True)
-    hidden = (jax.nn.silu(gate_act) * up_act).astype(jnp.bfloat16)
-    branch = lax.psum_scatter(
-        jnp.dot(hidden, down_full, preferred_element_type=jnp.float32)
-        .astype(jnp.bfloat16)
-        .astype(jnp.float32)
-        .astype(jnp.bfloat16),
-        "tp",
-        scatter_dimension=0,
-        tiled=True,
-    )
+    if not short:
+        gate_act = jnp.dot(
+            gathered,
+            lax.all_gather(w_gate, "sp", axis=0, tiled=True),
+            preferred_element_type=jnp.float32,
+        )
+        up_act = jnp.dot(
+            gathered,
+            lax.all_gather(w_up, "sp", axis=0, tiled=True),
+            preferred_element_type=jnp.float32,
+        )
+        hidden = (jax.nn.silu(gate_act) * up_act).astype(jnp.bfloat16)
+        down_full = lax.all_gather(w_down, "sp", axis=1, tiled=True)
+        partial = jnp.dot(hidden, down_full, preferred_element_type=jnp.float32)
+        branch = lax.psum_scatter(
+            partial.astype(jnp.bfloat16), "tp", scatter_dimension=0, tiled=True
+        )
+    else:
+        branch = ring_feed_forward(gathered, gate_blocks, up_blocks, down_blocks, resid.shape)
     return (middle.astype(jnp.float32) + rms_norm(branch, post_ffn_gain)).astype(jnp.bfloat16)
 
 
@@ -181,6 +277,7 @@
         P(),
     )
     out_specs = P(("sp", "tp"), None)
+
     return jax.shard_map(
         per_device, mesh=mesh, in_specs=in_specs, out_specs=out_specs, check_vma=False
     )

time: 439 us -> 306 us (0.70)
  waiting for transfers between devices: 297 us -> 124 us
  starting transfers between devices: 0.38 us -> 45.3 us
  blocking collectives: 66.8 us -> 40.1 us
  local copies, waits for them, and re-layouts: 6.82 us -> 20.9 us
  matrix products: 43.3 us -> 51.6 us
    all_gather x3 -> x0, waiting for transfers between devices: 218 us -> none  [the longest x1 93.2 us: per_device(): down_full = lax.all_gather(w_down, 'sp', axis=1, tiled=True)]
    ppermute x0 -> x26, waiting for transfers between devices: none -> 123 us  [the longest x11 64.3 us: ring_gather(): up = lax.ppermute(up, 'sp', ahead)]
    all_gather x2 -> x0, blocking collectives: 55.4 us -> none  [entering(): lax.all_gather(a.astype(kind), axis)]
    ppermute x0 -> x26, starting transfers between devices: none -> 45.2 us  [the longest x11 20 us: ring_gather(): up = lax.ppermute(up, 'sp', ahead)]
    reduce_scatter x1, waiting for transfers between devices: 42.9 us -> 0.01 us  [ring_feed_forward(): piece = lax.psum_scatter(part, 'tp', scatter_dimension=0, tiled=True)]
    all_gather x1, waiting for transfers between devices: 34.2 us -> 0.01 us  [per_device(): gathered = lax.all_gather(ffn_input, 'tp', axis=0, tiled=True)]
    all_to_all x0 -> x1, blocking collectives: none -> 28.7 us  [ring_feed_forward(): lax.all_to_all(shares, 'tp', split_axis=0, concat_axis=0, tiled=True)]
    dot_general x3 -> x7, matrix products: 33 us -> 41.4 us  [the longest x4 29.1 us: project(): part = jnp.dot(columns, weight, preferred_element_type=jnp.float32)]
  transfers between devices with their start and end apart: 6 -> 29, of which waited for: 5 -> 12; matrix products, arithmetic and copies ran while one was open for 8% -> 19% of each run, Pallas kernels for 0% -> 0%
where the time goes in v1:
time: 306 us; the launch traced here: 305 us
  waiting for transfers between devices  124 us (41%)
  matrix products  51.6 us (17%)
  starting transfers between devices  45.3 us (15%)
  blocking collectives  40.1 us (13%)
  local copies, waits for them, and re-layouts  20.9 us (7%)
  between operations  13.6 us (4%)
  other arithmetic  9.25 us (3%)
    ppermute x11, waiting for transfers between devices, ring_gather(): up = lax.ppermute(up, 'sp', ahead)  64.3 us
    ppermute x10, waiting for transfers between devices, ring_gather(): down = lax.ppermute(down, 'sp', behind)  55.7 us
    dot_general x4, matrix products, project(): part = jnp.dot(columns, weight, preferred_element_type=jnp.float32)  29.1 us
    all_to_all x1, blocking collectives, ring_feed_forward(): lax.all_to_all(shares, 'tp', split_axis=0, concat_axis=0, tiled=True)  28.7 us
    ppermute x11, starting transfers between devices, ring_gather(): up = lax.ppermute(up, 'sp', ahead)  20 us
    ppermute x5, starting transfers between devices, from_earlier(): lax.ppermute(packed, 'sp', [(i, i + distance) for i in range(count - dist...  18.5 us
    dot_general x2, matrix products, ring_feed_forward(): jnp.dot(hidden, wide, preferred_element_type=jnp.float32)  11.6 us
    all_to_all x1, blocking collectives, per_device(): lax.all_to_all(retained, 'tp', split_axis=0, concat_axis=1, tiled=True)  11.4 us
  transfers between devices with their start and end apart: 29, of which 12 were waited for; matrix products, arithmetic and copies ran while one was open for 19% of the time, Pallas kernels for 0%

profile of v1, /device:TPU:0, one launch (start us, length us, event | category | flops | bytes accessed | tf_op | source)
XLA Modules:
  0.0 305.0 jit_solution(2847208788821859762)
XLA Ops:
  11.7 9.5 %while.13 = (s32[]{:T(128)}, f32[2,128,128]{2,1,0:T(8,128)S(1)}, f32[2,2,512,128]{3,2,1,0:T(8,128)}, f32[2,2,512]{2,1,0:T(2,128)S(1)}, bf16[2,2,512,128]{3,1,2,0...) while((s32[]{:T(128)}, f32[2,128,128]{2,1,0:T(8,128)S(1)}, ...), condition=%wide.region_3.4_spmd.clone, body=%wide.region_0.3_spmd.clone.sunk | while | flops 507643936 | bytes 5702508 | solution.py:207
  22.0 4.9 %collective-permute-start = (f32[2,136,128]{2,1,0:T(8,128)}, f32[2,136,128]{2,1,0:T(8,128)S(1)}, u32[]{:S(2)}, u32[]{:S(2)}) collective-permute-start(f32[2,136,128]{2,1,0:T(8,128)} %pad_maximum_fusion.6), channel_id=1, source_target_pairs={{0,4},{4,8},{8,12},{12,16},{16,20},{20,24},{24,28},{1,5},{5,9},{9,... | collective-permute-start | bytes 417800 | tf_op jit(solution)/shard_map/ppermute | solution.py:30
  26.9 3.5 %collective-permute-start.1 = (f32[2,136,128]{2,1,0:T(8,128)}, f32[2,136,128]{2,1,0:T(8,128)S(1)}, u32[]{:S(2)}, u32[]{:S(2)}) collective-permute-start(f32[2,136,128]{2,1,0:T(8,128)} %pad_maximum_fusion.6), channel_id=1, source_target_pairs={{0,8},{4,12},{8,16},{12,20},{16,24},{20,28},{1,9},{5,13},{9,17},{1... | collective-permute-start | bytes 417800 | tf_op jit(solution)/shard_map/ppermute | solution.py:30
  33.3 4.3 %collective-permute-start.2 = (f32[2,136,128]{2,1,0:T(8,128)S(1)}, f32[2,136,128]{2,1,0:T(8,128)S(1)}, u32[]{:S(2)}, u32[]{:S(2)}) collective-permute-start(f32[2,136,128]{2,1,0:T(8,128)S(1)} %pad_maximum_fusion.7), channel_id=1, source_target_pairs={{0,8},{4,12},{8,16},{12,20},{16,24},{20,28},{1,9},{5,13},{9,17},{1... | collective-permute-start | bytes 417800 | tf_op jit(solution)/shard_map/ppermute | solution.py:30
  37.6 4.5 %collective-permute-start.3 = (f32[2,136,128]{2,1,0:T(8,128)S(1)}, f32[2,136,128]{2,1,0:T(8,128)S(1)}, u32[]{:S(2)}, u32[]{:S(2)}) collective-permute-start(f32[2,136,128]{2,1,0:T(8,128)S(1)} %pad_maximum_fusion.7), channel_id=1, source_target_pairs={{0,16},{4,20},{8,24},{12,28},{1,17},{5,21},{9,25},{13,29},{2,18},{... | collective-permute-start | bytes 417800 | tf_op jit(solution)/shard_map/ppermute | solution.py:30
  43.5 1.8 collective-permute-done.3
  48.5 11.4 %all_to_all.21 = bf16[4,256,256]{1,2,0:T(8,128)(2,1)S(1)} all-to-all(bf16[4,256,256]{1,2,0:T(8,128)(2,1)S(1)} %copy.52), channel_id=1, replica_groups=mesh['sp'=8,'tp'=4] {'tp'}, dimensions={0} | all-to-all | bytes 1048576 | tf_op jit(solution)/shard_map/all_to_all | solution.py:222
  59.9 1.8 fusion.69
  67.2 4.0 %collective-permute-start.5 = (bf16[256,1408]{1,0:T(8,128)(2,1)S(1)}, bf16[256,1408]{1,0:T(8,128)(2,1)S(1)}, u32[]{:S(2)}, u32[]{:S(2)}) collective-permute-start(bf16[256,1408]{1,0:T(8,128)(2,1)S(1)} %copy-done.10), channel_id=1, source_target_pairs={{0,8},{8,16},{16,24},{24,28},{28,20},{20,12},{12,4},{4,0},{1,9},{9... | collective-permute-start | bytes 2162696 | tf_op jit(solution)/shard_map/ppermute | solution.py:65
  73.2 14.5 %collective-permute-done.5 = bf16[256,1408]{1,0:T(8,128)(2,1)S(1)} collective-permute-done((bf16[256,1408]{1,0:T(8,128)(2,1)S(1)}, bf16[256,1408]{1,0:T(8,128)(2,1)S(1)}, u32[]{:S(2)}, u32[]{:S(2)}) %collective-permute-start.5) | collective-permute-done | bytes 720928 | tf_op jit(solution)/shard_map/ppermute | solution.py:65
  87.7 2.5 collective-permute-start.7
  90.2 15.5 %collective-permute-done.6 = bf16[256,1408]{1,0:T(8,128)(2,1)} collective-permute-done((bf16[256,1408]{1,0:T(8,128)(2,1)S(1)}, bf16[256,1408]{1,0:T(8,128)(2,1)}, u32[]{:S(2)}, u32[]{:S(2)}) %collective-permute-start.6) | collective-permute-done | bytes 720928 | tf_op jit(solution)/shard_map/ppermute | solution.py:68
  105.7 2.0 collective-permute-start.14
  107.8 10.8 %collective-permute-done.7 = bf16[256,1408]{1,0:T(8,128)(2,1)} collective-permute-done((bf16[256,1408]{1,0:T(8,128)(2,1)S(1)}, bf16[256,1408]{1,0:T(8,128)(2,1)}, u32[]{:S(2)}, u32[]{:S(2)}) %collective-permute-start.7) | collective-permute-done | bytes 720928 | tf_op jit(solution)/shard_map/ppermute | solution.py:65
  118.6 2.6 collective-permute-start.9
  121.2 2.0 collective-permute-start.19
  123.2 13.4 %collective-permute-done.8 = bf16[256,1408]{1,0:T(8,128)(2,1)} collective-permute-done((bf16[256,1408]{1,0:T(8,128)(2,1)}, bf16[256,1408]{1,0:T(8,128)(2,1)}, u32[]{:S(2)}, u32[]{:S(2)}) %collective-permute-start.8) | collective-permute-done | bytes 720928 | tf_op jit(solution)/shard_map/ppermute | solution.py:68
  136.6 2.0 collective-permute-start.16
  138.7 10.9 %collective-permute-done.9 = bf16[256,1408]{1,0:T(8,128)(2,1)} collective-permute-done((bf16[256,1408]{1,0:T(8,128)(2,1)}, bf16[256,1408]{1,0:T(8,128)(2,1)}, u32[]{:S(2)}, u32[]{:S(2)}) %collective-permute-start.9) | collective-permute-done | bytes 720928 | tf_op jit(solution)/shard_map/ppermute | solution.py:65
  149.6 2.5 collective-permute-start.11
  152.1 2.8 constant_dynamic-slice_fusion.4
  154.9 4.8 %fusion.17 = f32[1024,1408]{1,0:T(8,128)S(1)} fusion(bf16[256,1408]{1,0:T(8,128)(2,1)} %collective-permute-done.7, bf16[256,1408]{1,0:T(8,128)(2,1)} %collective-permute-done.6, bf16[256,1408]{1,0:T(8,128)(2,1)S(1)} %copy-done.14, bf16[256,1408]{1,0:T(8,128)(2,1)S(1)} %copy-done.10, bf16[1024,256]{1,0:T(8,128)(2,1)S(1)} %get-tuple-element.117, ...), kind=kOutput, calls=%fused_computation.38 | convolution fusion | flops 2972712960 | bytes 10747904 | tf_op jit(solution)/shard_map/dot_general | solution.py:148
  159.8 7.3 %fusion.33 = f32[1024,1408]{1,0:T(8,128)} fusion(bf16[256,1408]{1,0:T(8,128)(2,1)} %collective-permute-done.14, bf16[256,1408]{1,0:T(8,128)(2,1)S(1)} %copy-done.16, bf16[256,1408]{1,0:T(8,128)(2,1)} %collective-permute-done.12, bf16[256,1408]{1,0:T(8,128)(2,1)S(1)} %copy-done.11, bf16[1024,256]{1,0:T(8,128)(2,1)S(1)} %get-tuple-element.117, ...), kind=kOutput, calls=%fused_computation.54 | convolution fusion | flops 2972712960 | bytes 10747904 | tf_op jit(solution)/shard_map/dot_general | solution.py:148
  169.5 26.5 %collective-permute-done.11 = bf16[256,1408]{1,0:T(8,128)(2,1)} collective-permute-done((bf16[256,1408]{1,0:T(8,128)(2,1)}, bf16[256,1408]{1,0:T(8,128)(2,1)}, u32[]{:S(2)}, u32[]{:S(2)}) %collective-permute-start.11) | collective-permute-done | bytes 720928 | tf_op jit(solution)/shard_map/ppermute | solution.py:65
  195.9 7.7 %fusion.25 = f32[1024,1408]{1,0:T(8,128)} fusion(bf16[256,1408]{1,0:T(8,128)(2,1)} %collective-permute-done.11, bf16[256,1408]{1,0:T(8,128)(2,1)} %collective-permute-done.10, bf16[256,1408]{1,0:T(8,128)(2,1)} %collective-permute-done.9, bf16[256,1408]{1,0:T(8,128)(2,1)} %collective-permute-done.8, bf16[1024,256]{1,0:T(8,128)(2,1)S(1)} %get-tuple-element.113, ...), kind=kOutput, calls=%fused_computation.46 | convolution fusion | flops 2972712960 | bytes 10747904 | tf_op jit(solution)/shard_map/dot_general | solution.py:148
  203.7 9.3 %multiply_convert_fusion.3 = bf16[1024,1408]{1,0:T(8,128)(2,1)S(1)} fusion(f32[1024,1408]{1,0:T(8,128)} %fusion.33, f32[1024,1408]{1,0:T(8,128)S(1)} %fusion.17, f32[1024,1408]{1,0:T(8,128)} %fusion.25, bf16[256,1408]{1,0:T(8,128)(2,1)} %collective-permute-done.18, bf16[256,1408]{1,0:T(8,128)(2,1)} %collective-permute-done.17, ...), kind=kOutput, calls=%fused_computation.34 | convolution fusion | flops 2984247296 | bytes 25165824 | tf_op jit(solution)/shard_map/dot_general | solution.py:148
  214.5 5.9 %fusion.89 = bf16[1024,1024]{1,0:T(8,128)(2,1)} fusion(bf16[1024,1408]{1,0:T(8,128)(2,1)S(1)} %multiply_convert_fusion.3, bf16[1408,256]{1,0:T(8,128)(2,1)S(1)} %collective-permute-done.21, bf16[1408,256]{1,0:T(8,128)(2,1)S(1)} %collective-permute-done.20, bf16[1408,256]{1,0:T(8,128)(2,1)} %collective-permute-done.19, bf16[1408,256]{1,0:T(8,128)(2,1)S(1)} %copy-done.12), kind=kOutput, calls=%fused_computation.118 | convolution fusion | flops 2965372928 | bytes 7864320 | tf_op jit(solution)/shard_map/dot_general | solution.py:160
  220.4 2.0 collective-permute-start.22
  223.0 14.2 %collective-permute-done.22 = bf16[1408,256]{1,0:T(8,128)(2,1)S(1)} collective-permute-done((bf16[1408,256]{1,0:T(8,128)(2,1)S(1)}, bf16[1408,256]{1,0:T(8,128)(2,1)S(1)}, u32[]{:S(2)}, u32[]{:S(2)}) %collective-permute-start.22) | collective-permute-done | bytes 720928 | tf_op jit(solution)/shard_map/ppermute | solution.py:68
  239.3 12.6 %collective-permute-done.24 = bf16[1408,256]{1,0:T(8,128)(2,1)S(1)} collective-permute-done((bf16[1408,256]{1,0:T(8,128)(2,1)S(1)}, bf16[1408,256]{1,0:T(8,128)(2,1)S(1)}, u32[]{:S(2)}, u32[]{:S(2)}) %collective-permute-start.24) | collective-permute-done | bytes 720928 | tf_op jit(solution)/shard_map/ppermute | solution.py:68
  253.4 5.7 %fusion.86 = bf16[1024,1024]{1,0:T(8,128)(2,1)S(1)} fusion(bf16[1024,1408]{1,0:T(8,128)(2,1)} %copy-done.17, bf16[1408,256]{1,0:T(8,128)(2,1)S(1)} %collective-permute-done.25, bf16[1408,256]{1,0:T(8,128)(2,1)S(1)} %collective-permute-done.24, bf16[1408,256]{1,0:T(8,128)(2,1)S(1)} %collective-permute-done.23, bf16[1408,256]{1,0:T(8,128)(2,1)S(1)} %collective-permute-done.22), kind=kOutput, calls=%fused_computation.117 | convolution fusion | flops 2965372928 | bytes 7864320 | tf_op jit(solution)/shard_map/dot_general | solution.py:160
  259.1 28.7 %all_to_all.22 = bf16[4,256,1024]{2,1,0:T(8,128)(2,1)S(1)} all-to-all(bf16[4,256,1024]{2,1,0:T(8,128)(2,1)S(1)} %bitcast.121), channel_id=1, replica_groups=mesh['sp'=8,'tp'=4] {'tp'}, dimensions={0} | all-to-all | bytes 4194304 | tf_op jit(solution)/shard_map/all_to_all | solution.py:165
  (160 shorter events, 48.9 us)
Async XLA Ops:
  6.5 53.4 %all-gather.3.cloned.1.call-start = ((), (), s32[]{:S(2)}) async-start(), calls=%async_computation.3 | async-start | bytes 5242880 | tf_op jit(solution)/shard_map/all_gather | solution.py:226
  7.3 144.8 %all-gather.5.cloned.1.call-start = ((), (), s32[]{:S(2)}) async-start(), calls=%async_computation.4 | async-start | bytes 5242880 | tf_op jit(solution)/shard_map/all_gather | solution.py:239
  22.0 11.2 %collective-permute-start = (f32[2,136,128]{2,1,0:T(8,128)}, f32[2,136,128]{2,1,0:T(8,128)S(1)}, u32[]{:S(2)}, u32[]{:S(2)}) collective-permute-start(f32[2,136,128]{2,1,0:T(8,128)} %pad_maximum_fusion.6), channel_id=1, source_target_pairs={{0,4},{4,8},{8,12},{12,16},{16,20},{20,24},{24,28},{1,5},{5,9},{9,... | collective-permute-start | bytes 417800 | tf_op jit(solution)/shard_map/ppermute | solution.py:30
  26.9 6.4 %collective-permute-start.1 = (f32[2,136,128]{2,1,0:T(8,128)}, f32[2,136,128]{2,1,0:T(8,128)S(1)}, u32[]{:S(2)}, u32[]{:S(2)}) collective-permute-start(f32[2,136,128]{2,1,0:T(8,128)} %pad_maximum_fusion.6), channel_id=1, source_target_pairs={{0,8},{4,12},{8,16},{12,20},{16,24},{20,28},{1,9},{5,13},{9,17},{1... | collective-permute-start | bytes 417800 | tf_op jit(solution)/shard_map/ppermute | solution.py:30
  33.3 10.1 %collective-permute-start.2 = (f32[2,136,128]{2,1,0:T(8,128)S(1)}, f32[2,136,128]{2,1,0:T(8,128)S(1)}, u32[]{:S(2)}, u32[]{:S(2)}) collective-permute-start(f32[2,136,128]{2,1,0:T(8,128)S(1)} %pad_maximum_fusion.7), channel_id=1, source_target_pairs={{0,8},{4,12},{8,16},{12,20},{16,24},{20,28},{1,9},{5,13},{9,17},{1... | collective-permute-start | bytes 417800 | tf_op jit(solution)/shard_map/ppermute | solution.py:30
  37.6 7.6 %collective-permute-start.3 = (f32[2,136,128]{2,1,0:T(8,128)S(1)}, f32[2,136,128]{2,1,0:T(8,128)S(1)}, u32[]{:S(2)}, u32[]{:S(2)}) collective-permute-start(f32[2,136,128]{2,1,0:T(8,128)S(1)} %pad_maximum_fusion.7), channel_id=1, source_target_pairs={{0,16},{4,20},{8,24},{12,28},{1,17},{5,21},{9,25},{13,29},{2,18},{... | collective-permute-start | bytes 417800 | tf_op jit(solution)/shard_map/ppermute | solution.py:30
  42.2 4.6 %collective-permute-start.4 = (f32[2,136,128]{2,1,0:T(8,128)S(1)}, f32[2,136,128]{2,1,0:T(8,128)S(1)}, u32[]{:S(2)}, u32[]{:S(2)}) collective-permute-start(f32[2,136,128]{2,1,0:T(8,128)S(1)} %pad_maximum_fusion.7), channel_id=1, source_target_pairs={{0,24},{4,28},{1,25},{5,29},{2,26},{6,30},{3,27},{7,31}} | collective-permute-start | bytes 417800 | tf_op jit(solution)/shard_map/ppermute | solution.py:30
  65.1 56.1 %copy-start.12 = (bf16[1408,256]{1,0:T(8,128)(2,1)S(1)}, bf16[1408,256]{1,0:T(8,128)(2,1)}, u32[]{:S(2)}) copy-start(bf16[1408,256]{1,0:T(8,128)(2,1)} %param.28) | copy-start | bytes 2162692
  67.1 222.0 %reduce-scatter.2.cloned.1.call-start = ((), (), s32[]{:S(2)}) async-start(), calls=%async_computation.5 | async-start | bytes 2621440 | tf_op jit(solution)/shard_map/reduce_scatter | solution.py:162
  67.2 20.5 %collective-permute-start.5 = (bf16[256,1408]{1,0:T(8,128)(2,1)S(1)}, bf16[256,1408]{1,0:T(8,128)(2,1)S(1)}, u32[]{:S(2)}, u32[]{:S(2)}) collective-permute-start(bf16[256,1408]{1,0:T(8,128)(2,1)S(1)} %copy-done.10), channel_id=1, source_target_pairs={{0,8},{8,16},{16,24},{24,28},{28,20},{20,12},{12,4},{4,0},{1,9},{9... | collective-permute-start | bytes 2162696 | tf_op jit(solution)/shard_map/ppermute | solution.py:65
  71.2 19.0 %collective-permute-start.13 = (bf16[256,1408]{1,0:T(8,128)(2,1)S(1)}, bf16[256,1408]{1,0:T(8,128)(2,1)S(1)}, u32[]{:S(2)}, u32[]{:S(2)}) collective-permute-start(bf16[256,1408]{1,0:T(8,128)(2,1)S(1)} %copy-done.11), channel_id=1, source_target_pairs={{8,0},{16,8},{24,16},{28,24},{20,28},{12,20},{4,12},{0,4},{9,1},{1... | collective-permute-start | bytes 2162696 | tf_op jit(solution)/shard_map/ppermute | solution.py:68
  71.2 34.6 %collective-permute-start.6 = (bf16[256,1408]{1,0:T(8,128)(2,1)S(1)}, bf16[256,1408]{1,0:T(8,128)(2,1)}, u32[]{:S(2)}, u32[]{:S(2)}) collective-permute-start(bf16[256,1408]{1,0:T(8,128)(2,1)S(1)} %copy-done.10), channel_id=1, source_target_pairs={{8,0},{16,8},{24,16},{28,24},{20,28},{12,20},{4,12},{0,4},{9,1},{1... | collective-permute-start | bytes 2162696 | tf_op jit(solution)/shard_map/ppermute | solution.py:68
  72.8 33.0 %collective-permute-start.12 = (bf16[256,1408]{1,0:T(8,128)(2,1)S(1)}, bf16[256,1408]{1,0:T(8,128)(2,1)}, u32[]{:S(2)}, u32[]{:S(2)}) collective-permute-start(bf16[256,1408]{1,0:T(8,128)(2,1)S(1)} %copy-done.11), channel_id=1, source_target_pairs={{0,8},{8,16},{16,24},{24,28},{28,20},{20,12},{12,4},{4,0},{1,9},{9... | collective-permute-start | bytes 2162696 | tf_op jit(solution)/shard_map/ppermute | solution.py:65
  87.7 33.5 %copy-start.13 = (bf16[256,1408]{1,0:T(8,128)(2,1)}, bf16[256,1408]{1,0:T(8,128)(2,1)S(1)}, u32[]{:S(2)}) copy-start(bf16[256,1408]{1,0:T(8,128)(2,1)S(1)} %collective-permute-done.5) | copy-start | bytes 2162692
  87.7 30.9 %collective-permute-start.7 = (bf16[256,1408]{1,0:T(8,128)(2,1)S(1)}, bf16[256,1408]{1,0:T(8,128)(2,1)}, u32[]{:S(2)}, u32[]{:S(2)}) collective-permute-start(bf16[256,1408]{1,0:T(8,128)(2,1)S(1)} %collective-permute-done.5), channel_id=1, source_target_pairs={{0,8},{8,16},{16,24},{24,28},{28,20},{20,12},{12,4},{4,0},{1,9},{9... | collective-permute-start | bytes 2162696 | tf_op jit(solution)/shard_map/ppermute | solution.py:65
  90.2 31.0 %copy-start.15 = (bf16[256,1408]{1,0:T(8,128)(2,1)}, bf16[256,1408]{1,0:T(8,128)(2,1)S(1)}, u32[]{:S(2)}) copy-start(bf16[256,1408]{1,0:T(8,128)(2,1)S(1)} %collective-permute-done.13) | copy-start | bytes 2162692
  90.2 31.0 %collective-permute-start.15 = (bf16[256,1408]{1,0:T(8,128)(2,1)S(1)}, bf16[256,1408]{1,0:T(8,128)(2,1)}, u32[]{:S(2)}, u32[]{:S(2)}) collective-permute-start(bf16[256,1408]{1,0:T(8,128)(2,1)S(1)} %collective-permute-done.13), channel_id=1, source_target_pairs={{8,0},{16,8},{24,16},{28,24},{20,28},{12,20},{4,12},{0,4},{9,1},{1... | collective-permute-start | bytes 2162696 | tf_op jit(solution)/shard_map/ppermute | solution.py:68
  105.7 30.9 %collective-permute-start.8 = (bf16[256,1408]{1,0:T(8,128)(2,1)}, bf16[256,1408]{1,0:T(8,128)(2,1)}, u32[]{:S(2)}, u32[]{:S(2)}) collective-permute-start(bf16[256,1408]{1,0:T(8,128)(2,1)} %collective-permute-done.6), channel_id=1, source_target_pairs={{8,0},{16,8},{24,16},{28,24},{20,28},{12,20},{4,12},{0,4},{9,1},{1... | collective-permute-start | bytes 2162696 | tf_op jit(solution)/shard_map/ppermute | solution.py:68
  105.7 30.9 %collective-permute-start.14 = (bf16[256,1408]{1,0:T(8,128)(2,1)}, bf16[256,1408]{1,0:T(8,128)(2,1)}, u32[]{:S(2)}, u32[]{:S(2)}) collective-permute-start(bf16[256,1408]{1,0:T(8,128)(2,1)} %collective-permute-done.12), channel_id=1, source_target_pairs={{0,8},{8,16},{16,24},{24,28},{28,20},{20,12},{12,4},{4,0},{1,9},{9... | collective-permute-start | bytes 2162696 | tf_op jit(solution)/shard_map/ppermute | solution.py:65
  118.6 31.0 %collective-permute-start.9 = (bf16[256,1408]{1,0:T(8,128)(2,1)}, bf16[256,1408]{1,0:T(8,128)(2,1)}, u32[]{:S(2)}, u32[]{:S(2)}) collective-permute-start(bf16[256,1408]{1,0:T(8,128)(2,1)} %collective-permute-done.7), channel_id=1, source_target_pairs={{0,8},{8,16},{16,24},{24,28},{28,20},{20,12},{12,4},{4,0},{1,9},{9... | collective-permute-start | bytes 2162696 | tf_op jit(solution)/shard_map/ppermute | solution.py:65
  121.2 30.9 %collective-permute-start.17 = (bf16[256,1408]{1,0:T(8,128)(2,1)}, bf16[256,1408]{1,0:T(8,128)(2,1)}, u32[]{:S(2)}, u32[]{:S(2)}) collective-permute-start(bf16[256,1408]{1,0:T(8,128)(2,1)} %collective-permute-done.15), channel_id=1, source_target_pairs={{8,0},{16,8},{24,16},{28,24},{20,28},{12,20},{4,12},{0,4},{9,1},{1... | collective-permute-start | bytes 2162696 | tf_op jit(solution)/shard_map/ppermute | solution.py:68
  121.2 45.8 %collective-permute-start.19 = (bf16[1408,256]{1,0:T(8,128)(2,1)S(1)}, bf16[1408,256]{1,0:T(8,128)(2,1)}, u32[]{:S(2)}, u32[]{:S(2)}) collective-permute-start(bf16[1408,256]{1,0:T(8,128)(2,1)S(1)} %copy-done.12), channel_id=1, source_target_pairs={{0,8},{8,16},{16,24},{24,28},{28,20},{20,12},{12,4},{4,0},{1,9},{9... | collective-permute-start | bytes 2162696 | tf_op jit(solution)/shard_map/ppermute | solution.py:65
  136.6 31.9 %collective-permute-start.10 = (bf16[256,1408]{1,0:T(8,128)(2,1)}, bf16[256,1408]{1,0:T(8,128)(2,1)}, u32[]{:S(2)}, u32[]{:S(2)}) collective-permute-start(bf16[256,1408]{1,0:T(8,128)(2,1)} %collective-permute-done.8), channel_id=1, source_target_pairs={{8,0},{16,8},{24,16},{28,24},{20,28},{12,20},{4,12},{0,4},{9,1},{1... | collective-permute-start | bytes 2162696 | tf_op jit(solution)/shard_map/ppermute | solution.py:68
  136.6 67.0 %collective-permute-start.16 = (bf16[256,1408]{1,0:T(8,128)(2,1)}, bf16[256,1408]{1,0:T(8,128)(2,1)}, u32[]{:S(2)}, u32[]{:S(2)}) collective-permute-start(bf16[256,1408]{1,0:T(8,128)(2,1)} %collective-permute-done.14), channel_id=1, source_target_pairs={{0,8},{8,16},{16,24},{24,28},{28,20},{20,12},{12,4},{4,0},{1,9},{9... | collective-permute-start | bytes 2162696 | tf_op jit(solution)/shard_map/ppermute | solution.py:65
  149.6 46.3 %collective-permute-start.11 = (bf16[256,1408]{1,0:T(8,128)(2,1)}, bf16[256,1408]{1,0:T(8,128)(2,1)}, u32[]{:S(2)}, u32[]{:S(2)}) collective-permute-start(bf16[256,1408]{1,0:T(8,128)(2,1)} %collective-permute-done.9), channel_id=1, source_target_pairs={{0,8},{8,16},{16,24},{24,28},{28,20},{20,12},{12,4},{4,0},{1,9},{9... | collective-permute-start | bytes 2162696 | tf_op jit(solution)/shard_map/ppermute | solution.py:65
  152.1 51.6 %collective-permute-start.18 = (bf16[256,1408]{1,0:T(8,128)(2,1)}, bf16[256,1408]{1,0:T(8,128)(2,1)}, u32[]{:S(2)}, u32[]{:S(2)}) collective-permute-start(bf16[256,1408]{1,0:T(8,128)(2,1)} %collective-permute-done.17), channel_id=1, source_target_pairs={{8,0},{16,8},{24,16},{28,24},{20,28},{12,20},{4,12},{0,4},{9,1},{1... | collective-permute-start | bytes 2162696 | tf_op jit(solution)/shard_map/ppermute | solution.py:68
  167.0 46.0 %collective-permute-start.20 = (bf16[1408,256]{1,0:T(8,128)(2,1)S(1)}, bf16[1408,256]{1,0:T(8,128)(2,1)S(1)}, u32[]{:S(2)}, u32[]{:S(2)}) collective-permute-start(bf16[1408,256]{1,0:T(8,128)(2,1)S(1)} %copy-done.12), channel_id=1, source_target_pairs={{8,0},{16,8},{24,16},{28,24},{20,28},{12,20},{4,12},{0,4},{9,1},{1... | collective-permute-start | bytes 2162696 | tf_op jit(solution)/shard_map/ppermute | solution.py:68
  168.6 44.4 %collective-permute-start.21 = (bf16[1408,256]{1,0:T(8,128)(2,1)}, bf16[1408,256]{1,0:T(8,128)(2,1)S(1)}, u32[]{:S(2)}, u32[]{:S(2)}) collective-permute-start(bf16[1408,256]{1,0:T(8,128)(2,1)} %collective-permute-done.19), channel_id=1, source_target_pairs={{0,8},{8,16},{16,24},{24,28},{28,20},{20,12},{12,4},{4,0},{1,9},{9... | collective-permute-start | bytes 2162696 | tf_op jit(solution)/shard_map/ppermute | solution.py:65
  220.4 16.8 %collective-permute-start.22 = (bf16[1408,256]{1,0:T(8,128)(2,1)S(1)}, bf16[1408,256]{1,0:T(8,128)(2,1)S(1)}, u32[]{:S(2)}, u32[]{:S(2)}) collective-permute-start(bf16[1408,256]{1,0:T(8,128)(2,1)S(1)} %collective-permute-done.20), channel_id=1, source_target_pairs={{8,0},{16,8},{24,16},{28,24},{20,28},{12,20},{4,12},{0,4},{9,1},{1... | collective-permute-start | bytes 2162696 | tf_op jit(solution)/shard_map/ppermute | solution.py:68
  222.5 16.3 %collective-permute-start.23 = (bf16[1408,256]{1,0:T(8,128)(2,1)S(1)}, bf16[1408,256]{1,0:T(8,128)(2,1)S(1)}, u32[]{:S(2)}, u32[]{:S(2)}) collective-permute-start(bf16[1408,256]{1,0:T(8,128)(2,1)S(1)} %collective-permute-done.21), channel_id=1, source_target_pairs={{0,8},{8,16},{16,24},{24,28},{28,20},{20,12},{12,4},{4,0},{1,9},{9... | collective-permute-start | bytes 2162696 | tf_op jit(solution)/shard_map/ppermute | solution.py:65
  237.3 14.6 %collective-permute-start.24 = (bf16[1408,256]{1,0:T(8,128)(2,1)S(1)}, bf16[1408,256]{1,0:T(8,128)(2,1)S(1)}, u32[]{:S(2)}, u32[]{:S(2)}) collective-permute-start(bf16[1408,256]{1,0:T(8,128)(2,1)S(1)} %collective-permute-done.22), channel_id=1, source_target_pairs={{8,0},{16,8},{24,16},{28,24},{20,28},{12,20},{4,12},{0,4},{9,1},{1... | collective-permute-start | bytes 2162696 | tf_op jit(solution)/shard_map/ppermute | solution.py:68
  238.8 14.6 %collective-permute-start.25 = (bf16[1408,256]{1,0:T(8,128)(2,1)S(1)}, bf16[1408,256]{1,0:T(8,128)(2,1)S(1)}, u32[]{:S(2)}, u32[]{:S(2)}) collective-permute-start(bf16[1408,256]{1,0:T(8,128)(2,1)S(1)} %collective-permute-done.23), channel_id=1, source_target_pairs={{0,8},{8,16},{16,24},{24,28},{28,20},{20,12},{12,4},{4,0},{1,9},{9... | collective-permute-start | bytes 2162696 | tf_op jit(solution)/shard_map/ppermute | solution.py:65
  (15 other events, 86.3 us)
Sparse Core Ops, SparseCore 0:
  8.9 37.1 all-gather.2
  67.2 37.9 all-gather.4
  220.6 33.1 reduce-scatter.1

commit v2 on v1

--- a/solution.py
+++ b/solution.py
@@ -125,6 +125,26 @@
     normed = centered * lax.rsqrt(variance + EPSILON) * norm_gain[None]
     gate_vals = gates.astype(jnp.float32).reshape(normed.shape)
     return (jax.nn.silu(gate_vals) * normed).reshape(normed.shape[0], -1).astype(jnp.bfloat16)
+
+
+def share_sum(part, row_count):
+    count = lax.axis_size("tp")
+    if count != 4:
+        return lax.psum_scatter(part, "tp", scatter_dimension=0, tiled=True)
+    me = lax.axis_index("tp")
+    high, low = me // 2, me % 2
+    shares = part.reshape(2, 2, row_count, -1)
+
+    def swap(block, bit):
+        return lax.ppermute(block, "tp", [(i, i ^ bit) for i in range(count)])
+
+    def pick(block, index, dim):
+        return lax.dynamic_index_in_dim(block, index, dim, False)
+
+    nearer = swap(pick(shares, 1 - low, 1), 1).astype(jnp.float32)
+    pair = pick(shares, low, 1).astype(jnp.float32) + nearer
+    farther = swap(pick(pair, 1 - high, 0).astype(jnp.bfloat16), 2).astype(jnp.float32)
+    return (pick(pair, high, 0) + farther).astype(jnp.bfloat16)
 
 
 def ring_feed_forward(rows, gate_blocks, up_blocks, down_blocks, shape):
@@ -153,17 +173,12 @@
     up_act = project(up_blocks)
     hidden = (jax.nn.silu(gate_act) * up_act).astype(jnp.bfloat16)
     branch = jnp.zeros(shape, jnp.bfloat16)
-    for part_no, some in enumerate((down_blocks[:half], down_blocks[half:])):
+    for some in (down_blocks[:half], down_blocks[half:]):
         if not some:
             continue
         wide = jnp.concatenate([block for _, block in some], axis=1)
         part = jnp.dot(hidden, wide, preferred_element_type=jnp.float32).astype(jnp.bfloat16)
-        if part_no == 0:
-            piece = lax.psum_scatter(part, "tp", scatter_dimension=0, tiled=True)
-        else:
-            shares = part.reshape(lax.axis_size("tp"), shape[0], -1)
-            shares = lax.all_to_all(shares, "tp", split_axis=0, concat_axis=0, tiled=True)
-            piece = jnp.sum(shares.astype(jnp.float32), axis=0).astype(jnp.bfloat16)
+        piece = share_sum(part, shape[0])
         for slot, (offset, _) in enumerate(some):
             branch = lax.dynamic_update_slice_in_dim(
                 branch, piece[:, slot * width : (slot + 1) * width], owner_of(offset) * width, 1

time: 306 us -> 288 us (0.941)
  blocking collectives: 40.1 us -> 11.4 us
  starting transfers between devices: 45.3 us -> 53.9 us
  waiting for transfers between devices: 124 us -> 128 us
  other arithmetic: 9.25 us -> 13.1 us
  local copies, waits for them, and re-layouts: 20.9 us -> 17.5 us
    ppermute x10, waiting for transfers between devices: 55.7 us -> 17.6 us  [ring_gather(): down = lax.ppermute(down, 'sp', behind)]
    all_to_all x1 -> x0, blocking collectives: 28.7 us -> none  [ring_feed_forward(): lax.all_to_all(shares, 'tp', split_axis=0, concat_axis=0, tiled=True)]
    ppermute x11, waiting for transfers between devices: 64.3 us -> 85.6 us  [ring_gather(): up = lax.ppermute(up, 'sp', ahead)]
    ppermute x0 -> x4, waiting for transfers between devices: none -> 20.2 us  [swap(): return lax.ppermute(block, 'tp', [(i, i ^ bit) for i in range(count)])]
    dynamic_update_slice x8, local copies, waits for them, and re-layouts: 7.37 us -> 0.17 us  [ring_feed_forward(): lax.dynamic_update_slice_in_dim(branch, piece[:, slot * width:(slot + 1)...]
    ppermute x11, starting transfers between devices: 20 us -> 25.5 us  [ring_gather(): up = lax.ppermute(up, 'sp', ahead)]
    add x0 -> x2, other arithmetic: none -> 3.86 us  [share_sum(): pair = pick(shares, low, 1).astype(jnp.float32) + nearer]
  transfers between devices with their start and end apart: 29 -> 32, of which waited for: 12 -> 17; matrix products, arithmetic and copies ran while one was open for 19% -> 23% of each run, Pallas kernels for 0% -> 0%
where the time goes in v2:
time: 288 us; the launch traced here: 287 us
  waiting for transfers between devices  128 us (44%)
  starting transfers between devices  53.9 us (19%)
  matrix products  49.3 us (17%)
  local copies, waits for them, and re-layouts  17.5 us (6%)
  between operations  14 us (5%)
  other arithmetic  13.1 us (5%)
  blocking collectives  11.4 us (4%)
    ppermute x11, waiting for transfers between devices, ring_gather(): up = lax.ppermute(up, 'sp', ahead)  85.6 us
    dot_general x4, matrix products, project(): part = jnp.dot(columns, weight, preferred_element_type=jnp.float32)  28.1 us
    ppermute x11, starting transfers between devices, ring_gather(): up = lax.ppermute(up, 'sp', ahead)  25.5 us
    ppermute x4, waiting for transfers between devices, swap(): return lax.ppermute(block, 'tp', [(i, i ^ bit) for i in range(count)])  20.2 us
    ppermute x5, starting transfers between devices, from_earlier(): lax.ppermute(packed, 'sp', [(i, i + distance) for i in range(count - dist...  18.5 us
    ppermute x10, waiting for transfers between devices, ring_gather(): down = lax.ppermute(down, 'sp', behind)  17.6 us
    all_to_all x1, blocking collectives, per_device(): lax.all_to_all(retained, 'tp', split_axis=0, concat_axis=1, tiled=True)  11.4 us
    dot_general x2, matrix products, ring_feed_forward(): jnp.dot(hidden, wide, preferred_element_type=jnp.float32)  10.3 us
  transfers between devices with their start and end apart: 32, of which 17 were waited for; matrix products, arithmetic and copies ran while one was open for 23% of the time, Pallas kernels for 0%

profile of v2, /device:TPU:0, one launch (start us, length us, event | category | flops | bytes accessed | tf_op | source)
XLA Modules:
  0.0 287.0 jit_solution(12436995238273187082)
XLA Ops:
  11.7 9.5 %while.13 = (s32[]{:T(128)}, f32[2,128,128]{2,1,0:T(8,128)S(1)}, f32[2,2,512,128]{3,2,1,0:T(8,128)}, f32[2,2,512]{2,1,0:T(2,128)S(1)}, bf16[2,2,512,128]{3,1,2,0...) while((s32[]{:T(128)}, f32[2,128,128]{2,1,0:T(8,128)S(1)}, ...), condition=%wide.region_3.4_spmd.clone, body=%wide.region_0.3_spmd.clone.sunk | while | flops 507643936 | bytes 5702508 | solution.py:222
  22.0 4.9 %collective-permute-start = (f32[2,136,128]{2,1,0:T(8,128)}, f32[2,136,128]{2,1,0:T(8,128)S(1)}, u32[]{:S(2)}, u32[]{:S(2)}) collective-permute-start(f32[2,136,128]{2,1,0:T(8,128)} %pad_maximum_fusion.6), channel_id=1, source_target_pairs={{0,4},{4,8},{8,12},{12,16},{16,20},{20,24},{24,28},{1,5},{5,9},{9,... | collective-permute-start | bytes 417800 | tf_op jit(solution)/shard_map/ppermute | solution.py:30
  26.9 3.5 %collective-permute-start.1 = (f32[2,136,128]{2,1,0:T(8,128)}, f32[2,136,128]{2,1,0:T(8,128)S(1)}, u32[]{:S(2)}, u32[]{:S(2)}) collective-permute-start(f32[2,136,128]{2,1,0:T(8,128)} %pad_maximum_fusion.6), channel_id=1, source_target_pairs={{0,8},{4,12},{8,16},{12,20},{16,24},{20,28},{1,9},{5,13},{9,17},{1... | collective-permute-start | bytes 417800 | tf_op jit(solution)/shard_map/ppermute | solution.py:30
  33.3 4.3 %collective-permute-start.2 = (f32[2,136,128]{2,1,0:T(8,128)S(1)}, f32[2,136,128]{2,1,0:T(8,128)S(1)}, u32[]{:S(2)}, u32[]{:S(2)}) collective-permute-start(f32[2,136,128]{2,1,0:T(8,128)S(1)} %pad_maximum_fusion.7), channel_id=1, source_target_pairs={{0,8},{4,12},{8,16},{12,20},{16,24},{20,28},{1,9},{5,13},{9,17},{1... | collective-permute-start | bytes 417800 | tf_op jit(solution)/shard_map/ppermute | solution.py:30
  37.6 4.5 %collective-permute-start.3 = (f32[2,136,128]{2,1,0:T(8,128)S(1)}, f32[2,136,128]{2,1,0:T(8,128)S(1)}, u32[]{:S(2)}, u32[]{:S(2)}) collective-permute-start(f32[2,136,128]{2,1,0:T(8,128)S(1)} %pad_maximum_fusion.7), channel_id=1, source_target_pairs={{0,16},{4,20},{8,24},{12,28},{1,17},{5,21},{9,25},{13,29},{2,18},{... | collective-permute-start | bytes 417800 | tf_op jit(solution)/shard_map/ppermute | solution.py:30
  48.5 11.4 %all_to_all.16 = bf16[4,256,256]{1,2,0:T(8,128)(2,1)S(1)} all-to-all(bf16[4,256,256]{1,2,0:T(8,128)(2,1)S(1)} %copy.56), channel_id=1, replica_groups=mesh['sp'=8,'tp'=4] {'tp'}, dimensions={0} | all-to-all | bytes 1048576 | tf_op jit(solution)/shard_map/all_to_all | solution.py:237
  67.1 4.0 %collective-permute-start.5 = (bf16[256,1408]{1,0:T(8,128)(2,1)S(1)}, bf16[256,1408]{1,0:T(8,128)(2,1)S(1)}, u32[]{:S(2)}, u32[]{:S(2)}) collective-permute-start(bf16[256,1408]{1,0:T(8,128)(2,1)S(1)} %copy-done.12), channel_id=1, source_target_pairs={{0,8},{8,16},{16,24},{24,28},{28,20},{20,12},{12,4},{4,0},{1,9},{9... | collective-permute-start | bytes 2162696 | tf_op jit(solution)/shard_map/ppermute | solution.py:65
  71.1 2.0 collective-permute-start.12
  75.2 12.5 %collective-permute-done.5 = bf16[256,1408]{1,0:T(8,128)(2,1)S(1)} collective-permute-done((bf16[256,1408]{1,0:T(8,128)(2,1)S(1)}, bf16[256,1408]{1,0:T(8,128)(2,1)S(1)}, u32[]{:S(2)}, u32[]{:S(2)}) %collective-permute-start.5) | collective-permute-done | bytes 720928 | tf_op jit(solution)/shard_map/ppermute | solution.py:65
  92.2 10.9 %collective-permute-done.12 = bf16[256,1408]{1,0:T(8,128)(2,1)} collective-permute-done((bf16[256,1408]{1,0:T(8,128)(2,1)S(1)}, bf16[256,1408]{1,0:T(8,128)(2,1)}, u32[]{:S(2)}, u32[]{:S(2)}) %collective-permute-start.12) | collective-permute-done | bytes 720928 | tf_op jit(solution)/shard_map/ppermute | solution.py:65
  103.1 2.1 collective-permute-start.8
  107.2 11.3 %collective-permute-done.19 = bf16[1408,256]{1,0:T(8,128)(2,1)} collective-permute-done((bf16[1408,256]{1,0:T(8,128)(2,1)S(1)}, bf16[1408,256]{1,0:T(8,128)(2,1)}, u32[]{:S(2)}, u32[]{:S(2)}) %collective-permute-start.19) | collective-permute-done | bytes 720928 | tf_op jit(solution)/shard_map/ppermute | solution.py:65
  118.5 2.6 collective-permute-start.14
  123.8 10.2 %collective-permute-done.7 = bf16[256,1408]{1,0:T(8,128)(2,1)} collective-permute-done((bf16[256,1408]{1,0:T(8,128)(2,1)S(1)}, bf16[256,1408]{1,0:T(8,128)(2,1)}, u32[]{:S(2)}, u32[]{:S(2)}) %collective-permute-start.7) | collective-permute-done | bytes 720928 | tf_op jit(solution)/shard_map/ppermute | solution.py:65
  134.0 2.6 collective-permute-start.9
  136.6 15.4 %collective-permute-done.15 = bf16[256,1408]{1,0:T(8,128)(2,1)} collective-permute-done((bf16[256,1408]{1,0:T(8,128)(2,1)}, bf16[256,1408]{1,0:T(8,128)(2,1)}, u32[]{:S(2)}, u32[]{:S(2)}) %collective-permute-start.15) | collective-permute-done | bytes 720928 | tf_op jit(solution)/shard_map/ppermute | solution.py:68
  152.0 2.8 constant_dynamic-slice_fusion.4
  156.5 8.5 %collective-permute-done.21 = bf16[1408,256]{1,0:T(8,128)(2,1)} collective-permute-done((bf16[1408,256]{1,0:T(8,128)(2,1)}, bf16[1408,256]{1,0:T(8,128)(2,1)}, u32[]{:S(2)}, u32[]{:S(2)}) %collective-permute-start.21) | collective-permute-done | bytes 720928 | tf_op jit(solution)/shard_map/ppermute | solution.py:65
  165.0 2.5 collective-permute-start.25
  167.5 13.0 %collective-permute-done.9 = bf16[256,1408]{1,0:T(8,128)(2,1)} collective-permute-done((bf16[256,1408]{1,0:T(8,128)(2,1)}, bf16[256,1408]{1,0:T(8,128)(2,1)}, u32[]{:S(2)}, u32[]{:S(2)}) %collective-permute-start.9) | collective-permute-done | bytes 720928 | tf_op jit(solution)/shard_map/ppermute | solution.py:65
  180.4 2.5 collective-permute-start.11
  182.9 4.7 %fusion.17 = f32[1024,1408]{1,0:T(8,128)S(1)} fusion(bf16[256,1408]{1,0:T(8,128)(2,1)} %collective-permute-done.7, bf16[256,1408]{1,0:T(8,128)(2,1)} %collective-permute-done.6, bf16[256,1408]{1,0:T(8,128)(2,1)S(1)} %copy-done.18, bf16[256,1408]{1,0:T(8,128)(2,1)S(1)} %copy-done.12, bf16[1024,256]{1,0:T(8,128)(2,1)S(1)} %get-tuple-element.117, ...), kind=kOutput, calls=%fused_computation.38 | convolution fusion | flops 2972712960 | bytes 10747904 | tf_op jit(solution)/shard_map/dot_general | solution.py:168
  189.8 7.5 %fusion.33 = f32[1024,1408]{1,0:T(8,128)} fusion(bf16[256,1408]{1,0:T(8,128)(2,1)} %collective-permute-done.14, bf16[256,1408]{1,0:T(8,128)(2,1)} %collective-permute-done.13, bf16[256,1408]{1,0:T(8,128)(2,1)} %collective-permute-done.12, bf16[256,1408]{1,0:T(8,128)(2,1)S(1)} %copy-done.13, bf16[1024,256]{1,0:T(8,128)(2,1)S(1)} %get-tuple-element.117, ...), kind=kOutput, calls=%fused_computation.54 | convolution fusion | flops 2972712960 | bytes 10747904 | tf_op jit(solution)/shard_map/dot_general | solution.py:168
  198.3 2.0 collective-permute-start.27
  200.3 11.0 %collective-permute-done.11 = bf16[256,1408]{1,0:T(8,128)(2,1)S(1)} collective-permute-done((bf16[256,1408]{1,0:T(8,128)(2,1)}, bf16[256,1408]{1,0:T(8,128)(2,1)S(1)}, u32[]{:S(2)}, u32[]{:S(2)}) %collective-permute-start.11) | collective-permute-done | bytes 720928 | tf_op jit(solution)/shard_map/ppermute | solution.py:65
  211.3 7.3 %fusion.25 = f32[1024,1408]{1,0:T(8,128)} fusion(bf16[256,1408]{1,0:T(8,128)(2,1)S(1)} %collective-permute-done.11, bf16[256,1408]{1,0:T(8,128)(2,1)S(1)} %collective-permute-done.10, bf16[256,1408]{1,0:T(8,128)(2,1)} %collective-permute-done.9, bf16[256,1408]{1,0:T(8,128)(2,1)} %collective-permute-done.8, bf16[1024,256]{1,0:T(8,128)(2,1)S(1)} %get-tuple-element.113, ...), kind=kOutput, calls=%fused_computation.46 | convolution fusion | flops 2972712960 | bytes 10747904 | tf_op jit(solution)/shard_map/dot_general | solution.py:168
  218.6 8.2 %collective-permute-done.16 = bf16[256,1408]{1,0:T(8,128)(2,1)S(1)} collective-permute-done((bf16[256,1408]{1,0:T(8,128)(2,1)}, bf16[256,1408]{1,0:T(8,128)(2,1)S(1)}, u32[]{:S(2)}, u32[]{:S(2)}) %collective-permute-start.16) | collective-permute-done | bytes 720928 | tf_op jit(solution)/shard_map/ppermute | solution.py:65
  226.8 8.6 %multiply_convert_fusion.3 = bf16[1024,1408]{1,0:T(8,128)(2,1)} fusion(f32[1024,1408]{1,0:T(8,128)} %fusion.33, f32[1024,1408]{1,0:T(8,128)S(1)} %fusion.17, f32[1024,1408]{1,0:T(8,128)} %fusion.25, bf16[256,1408]{1,0:T(8,128)(2,1)S(1)} %collective-permute-done.18, bf16[256,1408]{1,0:T(8,128)(2,1)} %collective-permute-done.17, ...), kind=kOutput, calls=%fused_computation.34 | convolution fusion | flops 2984247296 | bytes 25165824 | tf_op jit(solution)/shard_map/dot_general | solution.py:168
  235.4 5.7 %fusion.89 = bf16[1024,1024]{1,0:T(8,128)(2,1)S(1)} fusion(bf16[1024,1408]{1,0:T(8,128)(2,1)} %multiply_convert_fusion.3, bf16[1408,256]{1,0:T(8,128)(2,1)} %collective-permute-done.21, bf16[1408,256]{1,0:T(8,128)(2,1)S(1)} %copy-done.16, bf16[1408,256]{1,0:T(8,128)(2,1)} %collective-permute-done.19, bf16[1408,256]{1,0:T(8,128)(2,1)S(1)} %copy-done.14), kind=kOutput, calls=%fused_computation.120 | convolution fusion | flops 2965372928 | bytes 7864320 | tf_op jit(solution)/shard_map/dot_general | solution.py:180
  242.5 4.5 %fusion.86 = bf16[1024,1024]{1,0:T(8,128)(2,1)S(1)} fusion(bf16[1024,1408]{1,0:T(8,128)(2,1)S(1)} %copy-done.19, bf16[1408,256]{1,0:T(8,128)(2,1)S(1)} %collective-permute-done.27, bf16[1408,256]{1,0:T(8,128)(2,1)S(1)} %collective-permute-done.26, bf16[1408,256]{1,0:T(8,128)(2,1)S(1)} %collective-permute-done.25, bf16[1408,256]{1,0:T(8,128)(2,1)} %collective-permute-done.24), kind=kOutput, calls=%fused_computation.119 | convolution fusion | flops 2965372928 | bytes 7864320 | tf_op jit(solution)/shard_map/dot_general | solution.py:180
  256.3 11.0 %collective-permute-done.23 = bf16[256,1024]{1,0:T(8,128)(2,1)} collective-permute-done((bf16[256,1024]{1,0:T(8,128)(2,1)}, bf16[256,1024]{1,0:T(8,128)(2,1)}, u32[]{:S(2)}, u32[]{:S(2)}) %collective-permute-start.23) | collective-permute-done | bytes 524320 | tf_op jit(solution)/shard_map/ppermute | solution.py:139
  268.8 9.2 %collective-permute-done.29 = bf16[256,1024]{1,0:T(8,128)(2,1)S(1)} collective-permute-done((bf16[256,1024]{1,0:T(8,128)(2,1)S(1)}, bf16[256,1024]{1,0:T(8,128)(2,1)S(1)}, u32[]{:S(2)}, u32[]{:S(2)}) %collective-permute-start.29) | collective-permute-done | bytes 524320 | tf_op jit(solution)/shard_map/ppermute | solution.py:139
  (175 shorter events, 61.6 us)
Async XLA Ops:
  6.5 53.4 %all-gather.3.cloned.1.call-start = ((), (), s32[]{:S(2)}) async-start(), calls=%async_computation.1 | async-start | bytes 5242880 | tf_op jit(solution)/shard_map/all_gather | solution.py:241
  7.3 144.8 %all-gather.5.cloned.1.call-start = ((), (), s32[]{:S(2)}) async-start(), calls=%async_computation.2 | async-start | bytes 5242880 | tf_op jit(solution)/shard_map/all_gather | solution.py:254
  22.0 11.2 %collective-permute-start = (f32[2,136,128]{2,1,0:T(8,128)}, f32[2,136,128]{2,1,0:T(8,128)S(1)}, u32[]{:S(2)}, u32[]{:S(2)}) collective-permute-start(f32[2,136,128]{2,1,0:T(8,128)} %pad_maximum_fusion.6), channel_id=1, source_target_pairs={{0,4},{4,8},{8,12},{12,16},{16,20},{20,24},{24,28},{1,5},{5,9},{9,... | collective-permute-start | bytes 417800 | tf_op jit(solution)/shard_map/ppermute | solution.py:30
  26.9 6.4 %collective-permute-start.1 = (f32[2,136,128]{2,1,0:T(8,128)}, f32[2,136,128]{2,1,0:T(8,128)S(1)}, u32[]{:S(2)}, u32[]{:S(2)}) collective-permute-start(f32[2,136,128]{2,1,0:T(8,128)} %pad_maximum_fusion.6), channel_id=1, source_target_pairs={{0,8},{4,12},{8,16},{12,20},{16,24},{20,28},{1,9},{5,13},{9,17},{1... | collective-permute-start | bytes 417800 | tf_op jit(solution)/shard_map/ppermute | solution.py:30
  33.3 10.1 %collective-permute-start.2 = (f32[2,136,128]{2,1,0:T(8,128)S(1)}, f32[2,136,128]{2,1,0:T(8,128)S(1)}, u32[]{:S(2)}, u32[]{:S(2)}) collective-permute-start(f32[2,136,128]{2,1,0:T(8,128)S(1)} %pad_maximum_fusion.7), channel_id=1, source_target_pairs={{0,8},{4,12},{8,16},{12,20},{16,24},{20,28},{1,9},{5,13},{9,17},{1... | collective-permute-start | bytes 417800 | tf_op jit(solution)/shard_map/ppermute | solution.py:30
  37.6 7.6 %collective-permute-start.3 = (f32[2,136,128]{2,1,0:T(8,128)S(1)}, f32[2,136,128]{2,1,0:T(8,128)S(1)}, u32[]{:S(2)}, u32[]{:S(2)}) collective-permute-start(f32[2,136,128]{2,1,0:T(8,128)S(1)} %pad_maximum_fusion.7), channel_id=1, source_target_pairs={{0,16},{4,20},{8,24},{12,28},{1,17},{5,21},{9,25},{13,29},{2,18},{... | collective-permute-start | bytes 417800 | tf_op jit(solution)/shard_map/ppermute | solution.py:30
  42.2 4.6 %collective-permute-start.4 = (f32[2,136,128]{2,1,0:T(8,128)S(1)}, f32[2,136,128]{2,1,0:T(8,128)S(1)}, u32[]{:S(2)}, u32[]{:S(2)}) collective-permute-start(f32[2,136,128]{2,1,0:T(8,128)S(1)} %pad_maximum_fusion.7), channel_id=1, source_target_pairs={{0,24},{4,28},{1,25},{5,29},{2,26},{6,30},{3,27},{7,31}} | collective-permute-start | bytes 417800 | tf_op jit(solution)/shard_map/ppermute | solution.py:30
  67.1 20.5 %collective-permute-start.5 = (bf16[256,1408]{1,0:T(8,128)(2,1)S(1)}, bf16[256,1408]{1,0:T(8,128)(2,1)S(1)}, u32[]{:S(2)}, u32[]{:S(2)}) collective-permute-start(bf16[256,1408]{1,0:T(8,128)(2,1)S(1)} %copy-done.12), channel_id=1, source_target_pairs={{0,8},{8,16},{16,24},{24,28},{28,20},{20,12},{12,4},{4,0},{1,9},{9... | collective-permute-start | bytes 2162696 | tf_op jit(solution)/shard_map/ppermute | solution.py:65
  71.1 19.1 %collective-permute-start.6 = (bf16[256,1408]{1,0:T(8,128)(2,1)S(1)}, bf16[256,1408]{1,0:T(8,128)(2,1)}, u32[]{:S(2)}, u32[]{:S(2)}) collective-permute-start(bf16[256,1408]{1,0:T(8,128)(2,1)S(1)} %copy-done.12), channel_id=1, source_target_pairs={{8,0},{16,8},{24,16},{28,24},{20,28},{12,20},{4,12},{0,4},{9,1},{1... | collective-permute-start | bytes 2162696 | tf_op jit(solution)/shard_map/ppermute | solution.py:68
  71.1 32.0 %collective-permute-start.12 = (bf16[256,1408]{1,0:T(8,128)(2,1)S(1)}, bf16[256,1408]{1,0:T(8,128)(2,1)}, u32[]{:S(2)}, u32[]{:S(2)}) collective-permute-start(bf16[256,1408]{1,0:T(8,128)(2,1)S(1)} %copy-done.13), channel_id=1, source_target_pairs={{0,8},{8,16},{16,24},{24,28},{28,20},{20,12},{12,4},{4,0},{1,9},{9... | collective-permute-start | bytes 2162696 | tf_op jit(solution)/shard_map/ppermute | solution.py:65
  73.2 32.5 %collective-permute-start.13 = (bf16[256,1408]{1,0:T(8,128)(2,1)S(1)}, bf16[256,1408]{1,0:T(8,128)(2,1)}, u32[]{:S(2)}, u32[]{:S(2)}) collective-permute-start(bf16[256,1408]{1,0:T(8,128)(2,1)S(1)} %copy-done.13), channel_id=1, source_target_pairs={{8,0},{16,8},{24,16},{28,24},{20,28},{12,20},{4,12},{0,4},{9,1},{1... | collective-permute-start | bytes 2162696 | tf_op jit(solution)/shard_map/ppermute | solution.py:68
  73.2 45.4 %collective-permute-start.19 = (bf16[1408,256]{1,0:T(8,128)(2,1)S(1)}, bf16[1408,256]{1,0:T(8,128)(2,1)}, u32[]{:S(2)}, u32[]{:S(2)}) collective-permute-start(bf16[1408,256]{1,0:T(8,128)(2,1)S(1)} %copy-done.14), channel_id=1, source_target_pairs={{0,8},{8,16},{16,24},{24,28},{28,20},{20,12},{12,4},{4,0},{1,9},{9... | collective-permute-start | bytes 2162696 | tf_op jit(solution)/shard_map/ppermute | solution.py:65
  87.7 33.5 %collective-permute-start.20 = (bf16[1408,256]{1,0:T(8,128)(2,1)S(1)}, bf16[1408,256]{1,0:T(8,128)(2,1)S(1)}, u32[]{:S(2)}, u32[]{:S(2)}) collective-permute-start(bf16[1408,256]{1,0:T(8,128)(2,1)S(1)} %copy-done.14), channel_id=1, source_target_pairs={{8,0},{16,8},{24,16},{28,24},{20,28},{12,20},{4,12},{0,4},{9,1},{1... | collective-permute-start | bytes 2162696 | tf_op jit(solution)/shard_map/ppermute | solution.py:68
  90.2 43.8 %collective-permute-start.7 = (bf16[256,1408]{1,0:T(8,128)(2,1)S(1)}, bf16[256,1408]{1,0:T(8,128)(2,1)}, u32[]{:S(2)}, u32[]{:S(2)}) collective-permute-start(bf16[256,1408]{1,0:T(8,128)(2,1)S(1)} %collective-permute-done.5), channel_id=1, source_target_pairs={{0,8},{8,16},{16,24},{24,28},{28,20},{20,12},{12,4},{4,0},{1,9},{9... | collective-permute-start | bytes 2162696 | tf_op jit(solution)/shard_map/ppermute | solution.py:65
  103.1 33.5 %collective-permute-start.8 = (bf16[256,1408]{1,0:T(8,128)(2,1)}, bf16[256,1408]{1,0:T(8,128)(2,1)}, u32[]{:S(2)}, u32[]{:S(2)}) collective-permute-start(bf16[256,1408]{1,0:T(8,128)(2,1)} %collective-permute-done.6), channel_id=1, source_target_pairs={{8,0},{16,8},{24,16},{28,24},{20,28},{12,20},{4,12},{0,4},{9,1},{1... | collective-permute-start | bytes 2162696 | tf_op jit(solution)/shard_map/ppermute | solution.py:68
  105.7 46.3 %collective-permute-start.15 = (bf16[256,1408]{1,0:T(8,128)(2,1)}, bf16[256,1408]{1,0:T(8,128)(2,1)}, u32[]{:S(2)}, u32[]{:S(2)}) collective-permute-start(bf16[256,1408]{1,0:T(8,128)(2,1)} %collective-permute-done.13), channel_id=1, source_target_pairs={{8,0},{16,8},{24,16},{28,24},{20,28},{12,20},{4,12},{0,4},{9,1},{1... | collective-permute-start | bytes 2162696 | tf_op jit(solution)/shard_map/ppermute | solution.py:68
  118.5 36.3 %collective-permute-start.14 = (bf16[256,1408]{1,0:T(8,128)(2,1)}, bf16[256,1408]{1,0:T(8,128)(2,1)}, u32[]{:S(2)}, u32[]{:S(2)}) collective-permute-start(bf16[256,1408]{1,0:T(8,128)(2,1)} %collective-permute-done.12), channel_id=1, source_target_pairs={{0,8},{8,16},{16,24},{24,28},{28,20},{20,12},{12,4},{4,0},{1,9},{9... | collective-permute-start | bytes 2162696 | tf_op jit(solution)/shard_map/ppermute | solution.py:65
  122.0 43.0 %collective-permute-start.21 = (bf16[1408,256]{1,0:T(8,128)(2,1)}, bf16[1408,256]{1,0:T(8,128)(2,1)}, u32[]{:S(2)}, u32[]{:S(2)}) collective-permute-start(bf16[1408,256]{1,0:T(8,128)(2,1)} %collective-permute-done.19), channel_id=1, source_target_pairs={{0,8},{8,16},{16,24},{24,28},{28,20},{20,12},{12,4},{4,0},{1,9},{9... | collective-permute-start | bytes 2162696 | tf_op jit(solution)/shard_map/ppermute | solution.py:65
  134.0 46.5 %collective-permute-start.9 = (bf16[256,1408]{1,0:T(8,128)(2,1)}, bf16[256,1408]{1,0:T(8,128)(2,1)}, u32[]{:S(2)}, u32[]{:S(2)}) collective-permute-start(bf16[256,1408]{1,0:T(8,128)(2,1)} %collective-permute-done.7), channel_id=1, source_target_pairs={{0,8},{8,16},{16,24},{24,28},{28,20},{20,12},{12,4},{4,0},{1,9},{9... | collective-permute-start | bytes 2162696 | tf_op jit(solution)/shard_map/ppermute | solution.py:65
  136.6 51.1 %collective-permute-start.24 = (bf16[1408,256]{1,0:T(8,128)(2,1)}, bf16[1408,256]{1,0:T(8,128)(2,1)}, u32[]{:S(2)}, u32[]{:S(2)}) collective-permute-start(bf16[1408,256]{1,0:T(8,128)(2,1)} %copy-done.15), channel_id=1, source_target_pairs={{8,0},{16,8},{24,16},{28,24},{20,28},{12,20},{4,12},{0,4},{9,1},{1... | collective-permute-start | bytes 2162696 | tf_op jit(solution)/shard_map/ppermute | solution.py:68
  152.0 37.2 %collective-permute-start.17 = (bf16[256,1408]{1,0:T(8,128)(2,1)}, bf16[256,1408]{1,0:T(8,128)(2,1)}, u32[]{:S(2)}, u32[]{:S(2)}) collective-permute-start(bf16[256,1408]{1,0:T(8,128)(2,1)} %collective-permute-done.15), channel_id=1, source_target_pairs={{8,0},{16,8},{24,16},{28,24},{20,28},{12,20},{4,12},{0,4},{9,1},{1... | collective-permute-start | bytes 2162696 | tf_op jit(solution)/shard_map/ppermute | solution.py:68
  154.8 43.4 %collective-permute-start.10 = (bf16[256,1408]{1,0:T(8,128)(2,1)}, bf16[256,1408]{1,0:T(8,128)(2,1)S(1)}, u32[]{:S(2)}, u32[]{:S(2)}) collective-permute-start(bf16[256,1408]{1,0:T(8,128)(2,1)} %collective-permute-done.8), channel_id=1, source_target_pairs={{8,0},{16,8},{24,16},{28,24},{20,28},{12,20},{4,12},{0,4},{9,1},{1... | collective-permute-start | bytes 2162696 | tf_op jit(solution)/shard_map/ppermute | solution.py:68
  165.0 33.3 %collective-permute-start.25 = (bf16[1408,256]{1,0:T(8,128)(2,1)}, bf16[1408,256]{1,0:T(8,128)(2,1)S(1)}, u32[]{:S(2)}, u32[]{:S(2)}) collective-permute-start(bf16[1408,256]{1,0:T(8,128)(2,1)} %collective-permute-done.21), channel_id=1, source_target_pairs={{0,8},{8,16},{16,24},{24,28},{28,20},{20,12},{12,4},{4,0},{1,9},{9... | collective-permute-start | bytes 2162696 | tf_op jit(solution)/shard_map/ppermute | solution.py:65
  180.4 30.9 %collective-permute-start.11 = (bf16[256,1408]{1,0:T(8,128)(2,1)}, bf16[256,1408]{1,0:T(8,128)(2,1)S(1)}, u32[]{:S(2)}, u32[]{:S(2)}) collective-permute-start(bf16[256,1408]{1,0:T(8,128)(2,1)} %collective-permute-done.9), channel_id=1, source_target_pairs={{0,8},{8,16},{16,24},{24,28},{28,20},{20,12},{12,4},{4,0},{1,9},{9... | collective-permute-start | bytes 2162696 | tf_op jit(solution)/shard_map/ppermute | solution.py:65
  187.7 39.1 %collective-permute-start.16 = (bf16[256,1408]{1,0:T(8,128)(2,1)}, bf16[256,1408]{1,0:T(8,128)(2,1)S(1)}, u32[]{:S(2)}, u32[]{:S(2)}) collective-permute-start(bf16[256,1408]{1,0:T(8,128)(2,1)} %collective-permute-done.14), channel_id=1, source_target_pairs={{0,8},{8,16},{16,24},{24,28},{28,20},{20,12},{12,4},{4,0},{1,9},{9... | collective-permute-start | bytes 2162696 | tf_op jit(solution)/shard_map/ppermute | solution.py:65
  189.2 37.6 %collective-permute-start.18 = (bf16[256,1408]{1,0:T(8,128)(2,1)}, bf16[256,1408]{1,0:T(8,128)(2,1)S(1)}, u32[]{:S(2)}, u32[]{:S(2)}) collective-permute-start(bf16[256,1408]{1,0:T(8,128)(2,1)} %collective-permute-done.17), channel_id=1, source_target_pairs={{8,0},{16,8},{24,16},{28,24},{20,28},{12,20},{4,12},{0,4},{9,1},{1... | collective-permute-start | bytes 2162696 | tf_op jit(solution)/shard_map/ppermute | solution.py:68
  198.3 43.0 %collective-permute-start.26 = (bf16[1408,256]{1,0:T(8,128)(2,1)}, bf16[1408,256]{1,0:T(8,128)(2,1)S(1)}, u32[]{:S(2)}, u32[]{:S(2)}) collective-permute-start(bf16[1408,256]{1,0:T(8,128)(2,1)} %collective-permute-done.24), channel_id=1, source_target_pairs={{8,0},{16,8},{24,16},{28,24},{20,28},{12,20},{4,12},{0,4},{9,1},{1... | collective-permute-start | bytes 2162696 | tf_op jit(solution)/shard_map/ppermute | solution.py:68
  198.3 44.2 %collective-permute-start.27 = (bf16[1408,256]{1,0:T(8,128)(2,1)S(1)}, bf16[1408,256]{1,0:T(8,128)(2,1)S(1)}, u32[]{:S(2)}, u32[]{:S(2)}) collective-permute-start(bf16[1408,256]{1,0:T(8,128)(2,1)S(1)} %collective-permute-done.25), channel_id=1, source_target_pairs={{0,8},{8,16},{16,24},{24,28},{28,20},{20,12},{12,4},{4,0},{1,9},{9... | collective-permute-start | bytes 2162696 | tf_op jit(solution)/shard_map/ppermute | solution.py:65
  241.2 8.1 %collective-permute-start.22 = (bf16[2,256,1024]{2,1,0:T(8,128)(2,1)S(1)}, bf16[2,256,1024]{2,1,0:T(8,128)(2,1)}, u32[]{:S(2)}, u32[]{:S(2)}) collective-permute-start(bf16[2,256,1024]{2,1,0:T(8,128)(2,1)S(1)} %dynamic-slice_bitcast_fusion.1), channel_id=1, source_target_pairs={{0,1},{1,0},{2,3},{3,2},{4,5},{5,4},{6,7},{7,6},{8,9},{9,8},{10,11... | collective-permute-start | bytes 3145736 | tf_op jit(solution)/shard_map/ppermute | solution.py:139
  249.4 3.2 %collective-permute-start.28 = (bf16[2,256,1024]{2,1,0:T(8,128)(2,1)}, bf16[2,256,1024]{2,1,0:T(8,128)(2,1)}, u32[]{:S(2)}, u32[]{:S(2)}) collective-permute-start(bf16[2,256,1024]{2,1,0:T(8,128)(2,1)} %dynamic-slice_bitcast_fusion), channel_id=1, source_target_pairs={{0,1},{1,0},{2,3},{3,2},{4,5},{5,4},{6,7},{7,6},{8,9},{9,8},{10,11... | collective-permute-start | bytes 3145736 | tf_op jit(solution)/shard_map/ppermute | solution.py:139
  252.2 15.1 %collective-permute-start.23 = (bf16[256,1024]{1,0:T(8,128)(2,1)}, bf16[256,1024]{1,0:T(8,128)(2,1)}, u32[]{:S(2)}, u32[]{:S(2)}) collective-permute-start(bf16[256,1024]{1,0:T(8,128)(2,1)} %fusion.100), channel_id=1, source_target_pairs={{0,2},{1,3},{2,0},{3,1},{4,6},{5,7},{6,4},{7,5},{8,10},{9,11},{10,... | collective-permute-start | bytes 1572872 | tf_op jit(solution)/shard_map/ppermute | solution.py:139
  254.6 23.4 %collective-permute-start.29 = (bf16[256,1024]{1,0:T(8,128)(2,1)S(1)}, bf16[256,1024]{1,0:T(8,128)(2,1)S(1)}, u32[]{:S(2)}, u32[]{:S(2)}) collective-permute-start(bf16[256,1024]{1,0:T(8,128)(2,1)S(1)} %fusion.101), channel_id=1, source_target_pairs={{0,2},{1,3},{2,0},{3,1},{4,6},{5,7},{6,4},{7,5},{8,10},{9,11},{10,... | collective-permute-start | bytes 1572872 | tf_op jit(solution)/shard_map/ppermute | solution.py:139
  (20 other events, 172.1 us)
Sparse Core Ops, SparseCore 0:
  8.9 37.1 all-gather.2
  67.2 37.9 all-gather.4
